TPU v7x, 128 devices: a whole 4x4x4 slice. The times are simulated.
128 devices in a mesh: ep: 16 (over z, x), tp: 8 (over y, core).
Axes of the slice: x: 4, y: 4, z: 4, core: 2. Of those that a mesh axis runs over, the one named last changes fastest.
Arguments:
- mixer_in: bfloat16 [16384, 2048], P(('ep', 'tp')), may hold values from -6 to 6
- expert_in: bfloat16 [65536, 2048], P(('ep', 'tp')), may hold values from -6 to 6
- mixer_gain: float32 [2048], replicated, may hold values from 0.1 to 1.9
- query_weight: bfloat16 [2048, 1024], replicated, may hold values from -0.125 to 0.125
- key_weight: bfloat16 [2048, 128], replicated, may hold values from -0.125 to 0.125
- value_weight: bfloat16 [2048, 128], replicated, may hold values from -0.125 to 0.125
- query_gain: float32 [64], replicated, may hold values from 0.4 to 6
- key_gain: float32 [64], replicated, may hold values from 0.4 to 6
- output_weight: bfloat16 [1024, 2048], replicated, may hold values from -0.1875 to 0.1875
- expert_gain: float32 [2048], replicated, may hold values from 0.1 to 1.9
- routes: int32 [65536, 2], P(('ep', 'tp')), may hold values from 0 to 31, all different within a row; in each aligned block of 512 rows (0 to 511, 512 to 1023, ...) at most 64 rows name the same one
- route_weight: float32 [65536, 2], P(('ep', 'tp')), may hold values from 0.2 to 1.5
- gate_weight: bfloat16 [32, 2048, 512], P('ep'), may hold values from -0.125 to 0.125
- up_weight: bfloat16 [32, 2048, 512], P('ep'), may hold values from -0.125 to 0.125
- down_weight: bfloat16 [32, 512, 2048], P('ep'), may hold values from -0.25 to 0.25
Outputs:
- mixer_out: bfloat16 [16384, 2048], P(('ep', 'tp'))
- expert_out: bfloat16 [65536, 2048], P(('ep', 'tp'))
Inputs may be any that keep to these rules, and one draw needn't show every extreme that they name: `routes`: each row names 2 different experts; among the rows of one device no expert is named more than 64 times, a bound that some block reaches.
All inputs are finite; a program needn't handle non-finite values.
Results may differ from a plain program's by a relative error of at most 0.0085.
The roundings to bfloat16 on the way count: a program that leaves them out, or rounds other values in their place, can miss the bound.
Values may be sent and summed in bfloat16 or wider, within the bound.
No kernel may reach another device: no remote copies, remote signals or barrier semaphores. Data moves between devices by JAX's collectives and lax.ppermute only.
A program may use at most 384 MiB of HBM per device.

v0:
```python
import math

import jax
import jax.numpy as jnp
from jax import lax
from jax.sharding import PartitionSpec as P

D = 2048
HEAD = 64
QHEADS = 16
KVHEADS = 2
GRID = 64
TOPK = 2
EXP_DEV = 2


eps = 1e-06
theta = 10000.0


def split_up(x, dim, count):
    before, after = (x.shape[:dim], x.shape[dim + 1 :])
    return jnp.moveaxis(x.reshape(*before, count, -1, *after), dim, 0)


def edges_of(length, count):
    unit = 8 if length >= 8 * count else 1
    return [length // unit * k // count * unit for k in range(1, count)]


def in_order(tiles, dim):
    lengths = list(tiles.shape[1:])
    lengths[dim] *= tiles.shape[0]
    return jnp.moveaxis(tiles, 0, dim).reshape(lengths)


def cut_exchange(x, axis, pieces, split_dim, concat_dim):
    tiles = split_up(x, split_dim, lax.axis_size(axis))
    widest = max(range(1, max(2, tiles.ndim - 1)), key=lambda d: tiles.shape[d])
    gathered = []
    for piece in jnp.split(tiles, edges_of(tiles.shape[widest], pieces), axis=widest):
        if piece.size:
            gathered.append(lax.all_to_all(piece, axis, split_axis=0, concat_axis=0, tiled=True))
    return in_order(jnp.concatenate(gathered, axis=widest), concat_dim)


def row_norm(values, gain):
    values = values.astype(jnp.float32)
    scaled = values * lax.rsqrt(jnp.mean(values * values, axis=-1, keepdims=True) + eps)
    return scaled * gain


def rotate(values, positions, grid):
    half = values.shape[-1] // 2
    freqs = half // 2
    inverse = theta ** (-(jnp.arange(freqs, dtype=jnp.float32) * 2.0) / half)
    grid_row = (positions // grid).astype(jnp.float32)
    grid_col = (positions % grid).astype(jnp.float32)
    angles = jnp.concatenate([grid_row[:, None] * inverse, grid_col[:, None] * inverse], axis=-1)
    cosine = jnp.cos(angles)[:, None, :]
    sine = jnp.sin(angles)[:, None, :]
    first = values[..., :half]
    second = values[..., half:]
    return jnp.concatenate(
        [first * cosine - second * sine, second * cosine + first * sine], axis=-1
    )


def project(
    rows, positions, mixer_gain, query_weight, key_weight, value_weight, query_gain, key_gain
):
    count = rows.shape[0]
    normed = row_norm(rows, mixer_gain).astype(jnp.bfloat16)
    queries = jnp.dot(normed, query_weight, preferred_element_type=jnp.float32).reshape(
        count, QHEADS, HEAD
    )
    keys = jnp.dot(normed, key_weight, preferred_element_type=jnp.float32).reshape(
        count, KVHEADS, HEAD
    )
    values = jnp.dot(normed, value_weight, preferred_element_type=jnp.float32).astype(jnp.bfloat16)
    queries = rotate(row_norm(queries, query_gain), positions, GRID).astype(jnp.bfloat16)
    keys = rotate(row_norm(keys, key_gain), positions, GRID).astype(jnp.bfloat16)
    return (queries, jnp.concatenate([keys.reshape(count, KVHEADS * HEAD), values], axis=1))


def per_device(
    mixer_in,
    expert_in,
    mixer_gain,
    query_weight,
    key_weight,
    value_weight,
    query_gain,
    key_gain,
    output_weight,
    expert_gain,
    routes,
    route_weight,
    gate_weight,
    up_weight,
    down_weight,
):
    own_rows = mixer_in.shape[0]
    offset = (lax.axis_index("ep") * lax.axis_size("tp") + lax.axis_index("tp")) * own_rows
    positions = offset + jnp.arange(own_rows, dtype=jnp.int32)
    queries, keyvals = project(
        mixer_in,
        positions,
        mixer_gain,
        query_weight,
        key_weight,
        value_weight,
        query_gain,
        key_gain,
    )
    groups = QHEADS // KVHEADS
    grouped = queries.reshape(own_rows, KVHEADS, groups, HEAD)
    scale = HEAD ** (-0.5)
    width = KVHEADS * HEAD
    start_state = (
        jnp.full((KVHEADS, groups, own_rows), -jnp.inf, jnp.float32),
        jnp.zeros((KVHEADS, groups, own_rows), jnp.float32),
        jnp.zeros((KVHEADS, groups, own_rows, HEAD), jnp.float32),
    )
    piece = lax.all_gather(keyvals, ("ep", "tp"), axis=0, tiled=True)
    rows = piece.shape[0]
    span = math.gcd(rows, 2048)
    blocks = piece.reshape(rows // span, span, 2 * width)

    def visit(state, block):
        peak, total, numer = state
        keys = block[:, :width].reshape(span, KVHEADS, HEAD)
        values = block[:, width:].reshape(span, KVHEADS, HEAD)
        scores = (
            jnp.einsum("rkgd,pkd->kgrp", grouped, keys, preferred_element_type=jnp.float32) * scale
        )
        fresh = jnp.maximum(peak, jnp.max(scores, axis=-1))
        factor = jnp.exp(peak - fresh)
        weights = jnp.exp(scores - fresh[..., None])
        total = total * factor + jnp.sum(weights, axis=-1)
        numer = numer * factor[..., None] + jnp.einsum(
            "kgrp,pkd->kgrd",
            weights.astype(jnp.bfloat16),
            values,
            preferred_element_type=jnp.float32,
        )
        return ((fresh, total, numer), None)

    state, _ = lax.scan(visit, start_state, blocks)
    peak, total, numer = state
    attended = jnp.transpose(numer / total[..., None], (2, 0, 1, 3)).reshape(
        own_rows, QHEADS * HEAD
    )
    mixer_out = jnp.dot(
        attended.astype(jnp.bfloat16), output_weight, preferred_element_type=jnp.float32
    ).astype(jnp.bfloat16)
    normed = row_norm(expert_in, expert_gain).astype(jnp.bfloat16)
    token_rows = routes.shape[0]
    experts = EXP_DEV * lax.axis_size("ep")
    capacity = 2 * token_rows * TOPK // experts
    flat = routes.reshape(-1)
    hot = (flat[:, None] == jnp.arange(experts, dtype=jnp.int32)[None, :]).astype(jnp.int32)
    rank = jnp.sum((jnp.cumsum(hot, axis=0) - hot) * hot, axis=-1)
    slot = flat * capacity + rank
    source = jnp.arange(flat.shape[0], dtype=jnp.int32) // TOPK
    table = jnp.full((experts * capacity,), token_rows, jnp.int32).at[slot].set(source)
    padded = jnp.concatenate([normed, jnp.zeros((1, D), jnp.bfloat16)], axis=0)
    outgoing = padded[table].reshape(experts, capacity, D)
    arrived = lax.all_to_all(outgoing, "ep", split_axis=0, concat_axis=1, tiled=True)
    gate = jnp.einsum("erd,edf->erf", arrived, gate_weight, preferred_element_type=jnp.float32)
    upper = jnp.einsum("erd,edf->erf", arrived, up_weight, preferred_element_type=jnp.float32)
    hidden = (jax.nn.silu(gate) * upper).astype(jnp.bfloat16)
    results = jnp.einsum(
        "erf,efd->erd", hidden, down_weight, preferred_element_type=jnp.float32
    ).astype(jnp.bfloat16)
    returned = cut_exchange(results, "ep", 2, 1, 0)
    picked = returned.reshape(experts * capacity, D)[slot].reshape(token_rows, TOPK, D)
    expert_out = jnp.sum(picked.astype(jnp.float32) * route_weight[..., None], axis=1).astype(
        jnp.bfloat16
    )
    return (mixer_out, expert_out)


def solution(mesh):
    placed = (
        P(("ep", "tp"), None),
        P(("ep", "tp"), None),
        P(),
        P(),
        P(),
        P(),
        P(),
        P(),
        P(),
        P(),
        P(("ep", "tp"), None),
        P(("ep", "tp"), None),
        P("ep", None, None),
        P("ep", None, None),
        P("ep", None, None),
    )
    return jax.shard_map(
        per_device,
        mesh=mesh,
        in_specs=placed,
        out_specs=(P(("ep", "tp"), None), P(("ep", "tp"), None)),
        check_vma=False,
    )
```

profile of v0, /device:TPU:16, one launch (start us, length us, event | category | flops | bytes accessed | tf_op | source)
XLA Modules:
  0.0 604.6 jit_solution(10277200398740517998)
XLA Ops:
  9.2 9.0 %reduce-window.6 = s32[32,8,128]{2,1,0:T(8,128)S(1)} reduce-window(s32[32,8,128]{2,1,0:T(8,128)S(1)} %fusion.19, s32[]{:T(128)} %constant.95.clone.1), window={size=1x1x128 pad=0_0x0_0x127_0}, to_apply=%region_8.9 | reduce-window | flops 4161536 | bytes 262148 | tf_op jit(solution)/shard_map/reduce-window
  26.4 11.0 %gather_fusion = bf16[2048,2048]{1,0:T(8,128)(2,1)} fusion(bf16[513,2048]{1,0:T(8,128)(2,1)S(1)} %concatenate.40, s32[2048]{0:T(1024)S(1)} %fusion.22), kind=kCustom, calls=%fused_computation | custom fusion | bytes 16785408 | tf_op jit(solution)/shard_map/gather | solution.py:168
  47.7 122.4 %all-to-all-done = bf16[32,64,2048]{2,1,0:T(8,128)(2,1)} async-done(((bf16[32,64,2048]{2,1,0:T(8,128)(2,1)}), bf16[32,64,2048]{2,1,0:T(8,128)(2,1)}, u32[]{:S(2)}, u32[]{:S(2)}) %all-to-all-start) | async-done | bytes 8388640 | tf_op jit(solution)/shard_map/all_to_all | solution.py:169
  170.2 8.8 %copy.44 = bf16[2,16,64,2048]{3,2,1,0:T(8,128)(2,1)} copy(bf16[2,16,64,2048]{3,2,0,1:T(8,128)(2,1)} %bitcast.13) | data formatting | bytes 16777216 | tf_op jit(solution)/shard_map/all_to_all | solution.py:169
  178.9 11.7 %fusion.38 = f32[2,1024,512]{2,1,0:T(8,128)} fusion(bf16[2,1024,2048]{2,1,0:T(8,128)(2,1)} %bitcast.108, bf16[2,2048,512]{2,1,0:T(8,128)(2,1)} %param.29), kind=kOutput, calls=%fused_computation.92 | convolution fusion | flops 4294967296 | bytes 16777216 | tf_op jit(solution)/shard_map/erd,edf->erf/dot_general | solution.py:170
  190.7 15.3 %convolution_convert_fusion = bf16[2,1024,2048]{2,1,0:T(8,128)(2,1)} fusion(bf16[2,512,2048]{2,1,0:T(8,128)(2,1)} %param.31, f32[2,1024,512]{2,1,0:T(8,128)} %fusion.38, bf16[2,1024,2048]{2,1,0:T(8,128)(2,1)} %bitcast.109, bf16[2,2048,512]{2,1,0:T(8,128)(2,1)} %param.30), kind=kOutput, calls=%fused_computation.21 | convolution fusion | flops 8600420352 | bytes 29360128 | tf_op jit(solution)/shard_map/erf,efd->erd/dot_general | solution.py:173
  206.0 8.3 %copy.57 = bf16[2,16,64,2048]{3,2,0,1:T(8,128)(2,1)} copy(bf16[2,16,64,2048]{3,2,1,0:T(8,128)(2,1)} %bitcast.110) | data formatting | bytes 16777216 | tf_op jit(solution)/shard_map/reshape | solution.py:23
  219.6 55.4 %all_to_all.28 = bf16[16,2,32,2048]{3,2,1,0:T(8,128)(2,1)} all-to-all(bf16[16,2,32,2048]{3,2,1,0:T(8,128)(2,1)S(1)} %get-tuple-element.94), channel_id=1, replica_groups=mesh['ep'=16,'tp'=8] {'ep'}, dimensions={0} | all-to-all | bytes 8388608 | tf_op jit(solution)/shard_map/all_to_all | solution.py:43
  284.4 51.3 %all-to-all-done.2 = bf16[16,2,32,2048]{3,2,1,0:T(8,128)(2,1)} async-done(((bf16[16,2,32,2048]{3,2,1,0:T(8,128)(2,1)}), bf16[16,2,32,2048]{3,2,1,0:T(8,128)(2,1)}, u32[]{:S(2)}, u32[]{:S(2)}) %all-to-all-start.2) | async-done | bytes 4194336 | tf_op jit(solution)/shard_map/all_to_all | solution.py:43
  335.7 8.3 %pad_maximum_fusion = bf16[16,2,64,2048]{3,2,1,0:T(8,128)(2,1)} fusion(bf16[16,2,32,2048]{3,2,1,0:T(8,128)(2,1)} %all-to-all-done.2, bf16[16,2,32,2048]{3,2,1,0:T(8,128)(2,1)} %all_to_all.28), kind=kLoop, calls=%fused_computation.18 | loop fusion | flops 16777216 | bytes 16777216 | tf_op jit(solution)/shard_map/concatenate | solution.py:44
  344.1 13.3 %gather_fusion.1 = bf16[1024,2048]{1,0:T(8,128)(2,1)} fusion(bf16[2048,2048]{1,0:T(8,128)(2,1)} %bitcast.101, s32[1024]{0:T(1024)S(1)} %broadcast_clamp_fusion), kind=kCustom, calls=%fused_computation.1 | custom fusion | bytes 8392704 | tf_op jit(solution)/shard_map/gather | solution.py:177
  357.3 9.7 %reshape.225 = f32[512,2,2048]{2,1,0:T(2,128)} reshape(bf16[1024,2048]{1,0:T(8,128)(2,1)} %gather_fusion.1) | data formatting | bytes 12582912 | tf_op jit(solution)/shard_map/convert_element_type | solution.py:178
  367.1 15.0 %multiply_reduce_fusion = bf16[512,2048]{1,0:T(8,128)(2,1)} fusion(f32[512,2,2048]{2,1,0:T(2,128)} %reshape.225, f32[512,2]{1,0:T(8,128)S(1)} %copy.46), kind=kLoop, calls=%fused_computation.20 | loop fusion | flops 3145728 | bytes 10489856 | tf_op jit(solution)/shard_map/reduce_sum | solution.py:178
  382.1 8.3 %copy.56 = bf16[32,8,8,2048]{3,2,0,1:T(8,128)(2,1)} copy(bf16[32,8,8,2048]{3,2,1,0:T(8,128)(2,1)} %bitcast.107) | data formatting | bytes 16777216 | tf_op jit(solution)/shard_map/reshape | solution.py:128
  390.3 203.5 %while.15 = (s32[]{:T(128)}, f32[2,8,128]{2,1,0:T(8,128)S(1)}, f32[2,8,128]{2,1,0:T(8,128)S(1)}, f32[2,8,128,64]{2,3,1,0:T(8,128)S(1)}, bf16[8,2048,256]{1,2,0:T...) while((s32[]{:T(128)}, f32[2,8,128]{2,1,0:T(8,128)S(1)}, ...), condition=%wide.region_6.7_spmd.clone, body=%wide.region_3.6_spmd.clone.sunk | while | flops 1107699712 | bytes 57016416 | solution.py:149
  399.8 8.6 %fusion.65 = f32[2,8,128]{2,1,0:T(8,128)S(1)} fusion(f32[2,2048,128,8]{2,1,3,0:T(8,128)} %get-tuple-element.155, f32[2,8,128]{2,1,0:T(8,128)S(1)} %select_maximum_fusion.2), kind=kLoop, calls=%fused_computation.7.clone.1 | loop fusion | flops 12580864 | bytes 16793600 | tf_op jit(solution)/shard_map/while/body/eval_jaxpr/reduce_sum | solution.py:140
  425.3 8.6 %fusion.65 = f32[2,8,128]{2,1,0:T(8,128)S(1)} fusion(f32[2,2048,128,8]{2,1,3,0:T(8,128)} %get-tuple-element.155, f32[2,8,128]{2,1,0:T(8,128)S(1)} %select_maximum_fusion.2), kind=kLoop, calls=%fused_computation.7.clone.1 | loop fusion | flops 12580864 | bytes 16793600 | tf_op jit(solution)/shard_map/while/body/eval_jaxpr/reduce_sum | solution.py:140
  450.7 8.6 %fusion.65 = f32[2,8,128]{2,1,0:T(8,128)S(1)} fusion(f32[2,2048,128,8]{2,1,3,0:T(8,128)} %get-tuple-element.155, f32[2,8,128]{2,1,0:T(8,128)S(1)} %select_maximum_fusion.2), kind=kLoop, calls=%fused_computation.7.clone.1 | loop fusion | flops 12580864 | bytes 16793600 | tf_op jit(solution)/shard_map/while/body/eval_jaxpr/reduce_sum | solution.py:140
  468.1 8.1 %bitcast_reduce_fusion.2 = (f32[2,8,128]{2,1,0:T(8,128)S(1)}, f32[2,2048,128,8]{2,1,3,0:T(8,128)}) fusion(bf16[2048,2,64,1]{0,2,3,1:T(8,128)(2,1)S(1)} %bitcast.102, bf16[128,2,8,64]{0,3,2,1:T(8,128)(2,1)S(1)} %get-tuple-element.180), kind=kOutput, calls=%fused_computation.4.clone.1 | convolution fusion | flops 545257472 | bytes 17571840 | tf_op jit(solution)/shard_map/while/body/eval_jaxpr/rkgd,pkd->kgrp/dot_general | solution.py:135
  476.2 8.6 %fusion.65 = f32[2,8,128]{2,1,0:T(8,128)S(1)} fusion(f32[2,2048,128,8]{2,1,3,0:T(8,128)} %get-tuple-element.155, f32[2,8,128]{2,1,0:T(8,128)S(1)} %select_maximum_fusion.2), kind=kLoop, calls=%fused_computation.7.clone.1 | loop fusion | flops 12580864 | bytes 16793600 | tf_op jit(solution)/shard_map/while/body/eval_jaxpr/reduce_sum | solution.py:140
  501.6 8.6 %fusion.65 = f32[2,8,128]{2,1,0:T(8,128)S(1)} fusion(f32[2,2048,128,8]{2,1,3,0:T(8,128)} %get-tuple-element.155, f32[2,8,128]{2,1,0:T(8,128)S(1)} %select_maximum_fusion.2), kind=kLoop, calls=%fused_computation.7.clone.1 | loop fusion | flops 12580864 | bytes 16793600 | tf_op jit(solution)/shard_map/while/body/eval_jaxpr/reduce_sum | solution.py:140
  527.0 8.6 %fusion.65 = f32[2,8,128]{2,1,0:T(8,128)S(1)} fusion(f32[2,2048,128,8]{2,1,3,0:T(8,128)} %get-tuple-element.155, f32[2,8,128]{2,1,0:T(8,128)S(1)} %select_maximum_fusion.2), kind=kLoop, calls=%fused_computation.7.clone.1 | loop fusion | flops 12580864 | bytes 16793600 | tf_op jit(solution)/shard_map/while/body/eval_jaxpr/reduce_sum | solution.py:140
  552.5 8.6 %fusion.65 = f32[2,8,128]{2,1,0:T(8,128)S(1)} fusion(f32[2,2048,128,8]{2,1,3,0:T(8,128)} %get-tuple-element.155, f32[2,8,128]{2,1,0:T(8,128)S(1)} %select_maximum_fusion.2), kind=kLoop, calls=%fused_computation.7.clone.1 | loop fusion | flops 12580864 | bytes 16793600 | tf_op jit(solution)/shard_map/while/body/eval_jaxpr/reduce_sum | solution.py:140
  577.9 8.6 %fusion.65 = f32[2,8,128]{2,1,0:T(8,128)S(1)} fusion(f32[2,2048,128,8]{2,1,3,0:T(8,128)} %get-tuple-element.155, f32[2,8,128]{2,1,0:T(8,128)S(1)} %select_maximum_fusion.2), kind=kLoop, calls=%fused_computation.7.clone.1 | loop fusion | flops 12580864 | bytes 16793600 | tf_op jit(solution)/shard_map/while/body/eval_jaxpr/reduce_sum | solution.py:140
  (128 shorter events, 165.2 us)
Async XLA Ops:
  7.2 38.9 %copy-start = (bf16[2048,128]{1,0:T(8,128)(2,1)S(1)}, bf16[2048,128]{1,0:T(8,128)(2,1)}, u32[]{:S(2)}) copy-start(bf16[2048,128]{1,0:T(8,128)(2,1)} %param.21) | copy-start | bytes 1572868
  7.2 18.4 %copy-start.2 = (bf16[512,2048]{1,0:T(8,128)(2,1)S(1)}, bf16[512,2048]{1,0:T(8,128)(2,1)}, u32[]{:S(2)}) copy-start(bf16[512,2048]{1,0:T(8,128)(2,1)} %param.18) | copy-start | bytes 6291460
  7.2 18.4 %copy-start.4 = (f32[2048]{0:T(1024)S(1)}, f32[2048]{0:T(1024)}, u32[]{:S(2)}) copy-start(f32[2048]{0:T(1024)} %param.26) | copy-start | bytes 24580
  37.4 8.5 %copy-start.3 = (bf16[128,2048]{1,0:T(8,128)(2,1)S(1)}, bf16[128,2048]{1,0:T(8,128)(2,1)}, u32[]{:S(2)}) copy-start(bf16[128,2048]{1,0:T(8,128)(2,1)} %param.17) | copy-start | bytes 1572868
  37.4 8.7 %copy-start.5 = (f32[2048]{0:T(1024)S(1)}, f32[2048]{0:T(1024)}, u32[]{:S(2)}) copy-start(f32[2048]{0:T(1024)} %param.19) | copy-start | bytes 24580
  37.4 9.2 %copy-start.7 = (f32[64]{0:T(128)S(1)}, f32[64]{0:T(128)}, u32[]{:S(2)}) copy-start(f32[64]{0:T(128)} %param.24) | copy-start | bytes 772
  37.4 9.3 %copy-start.9 = (bf16[2048,128]{1,0:T(8,128)(2,1)S(1)}, bf16[2048,128]{1,0:T(8,128)(2,1)}, u32[]{:S(2)}) copy-start(bf16[2048,128]{1,0:T(8,128)(2,1)} %param.22) | copy-start | bytes 1572868
  37.4 132.8 %all-to-all-start = ((bf16[32,64,2048]{2,1,0:T(8,128)(2,1)}), bf16[32,64,2048]{2,1,0:T(8,128)(2,1)}, u32[]{:S(2)}, u32[]{:S(2)}) async-start(bf16[32,64,2048]{2,1,0:T(8,128)(2,1)} %bitcast.104), calls=%async_computation | async-start | bytes 16777216 | tf_op jit(solution)/shard_map/all_to_all | solution.py:169
  45.5 336.6 %all-gather.2.cloned.1.call-start = ((), (), s32[]{:S(2)}) async-start(), calls=%async_computation.3 | async-start | bytes 8454144 | tf_op jit(solution)/shard_map/all_gather | solution.py:125
  275.0 4.9 copy-start.6
  275.0 60.7 %all-to-all-start.2 = ((bf16[16,2,32,2048]{3,2,1,0:T(8,128)(2,1)}), bf16[16,2,32,2048]{3,2,1,0:T(8,128)(2,1)}, u32[]{:S(2)}, u32[]{:S(2)}) async-start(bf16[16,2,32,2048]{3,2,1,0:T(8,128)(2,1)} %get-tuple-element.95), calls=%async_computation.2 | async-start | bytes 8388608 | tf_op jit(solution)/shard_map/all_to_all | solution.py:43
  279.9 4.2 copy-start.8
  593.9 3.8 copy-start.1
Sparse Core Ops, SparseCore 0:
  49.7 148.1 all-gather.1
where the time goes:
time: 606 us; the launch traced here: 605 us
  waiting for transfers between devices  174 us (29%)
  matrix products  159 us (26%)
  other arithmetic  106 us (17%)
  local copies, waits for them, and re-layouts  82.4 us (14%)
  blocking collectives  55.4 us (9%)
  between operations  14.4 us (2%)
  starting transfers between devices  13.2 us (2%)
    all_to_all x1, waiting for transfers between devices, per_device(): lax.all_to_all(outgoing, 'ep', split_axis=0, concat_axis=1, tiled=True)  122 us
    reduce_sum x8, other arithmetic, visit(): total = total * factor + jnp.sum(weights, axis=-1)  68.5 us
    dot_general x8, matrix products, visit(): jnp.einsum('rkgd,pkd->kgrp', grouped, keys, preferred_element_type=jnp.fl...  64.7 us
    dot_general x8, matrix products, visit(): jnp.einsum('kgrp,pkd->kgrd', weights.astype(jnp.bfloat16), values, prefer...  58.6 us
    all_to_all x1, blocking collectives, cut_exchange(): lax.all_to_all(piece, axis, split_axis=0, concat_axis=0, tiled=True)  55.4 us
    all_to_all x1, waiting for transfers between devices, cut_exchange(): lax.all_to_all(piece, axis, split_axis=0, concat_axis=0, tiled=True)  51.3 us
    dot_general x1, matrix products, per_device(): jnp.einsum('erf,efd->erd', hidden, down_weight, preferred_element_type=jn...  15.3 us
    reduce_sum x1, other arithmetic, per_device(): jnp.sum(picked.astype(jnp.float32) * route_weight[..., None], axis=1)  15 us
  transfers between devices with their start and end apart: 3, of which 2 were waited for; matrix products, arithmetic and copies ran while one was open for 17% of the time, Pallas kernels for 0%

commit v1 on v0

v1 whole, which is shorter than its diff:
```python
import functools

import jax
import jax.numpy as jnp
from jax import lax
from jax.experimental import pallas as pl
from jax.experimental.pallas import tpu as pltpu
from jax.sharding import PartitionSpec as P


D = 2048
HEAD = 64
QHEADS = 16
KVHEADS = 2
GRID = 64
FF = 512
EXP_DEV = 2
CAP = 64
LANES = 128
KEY_BLOCK = 2048
ROW_TILE = 256
VMEM = 56 * 1024 * 1024

eps = 1e-06
theta = 10000.0

f32 = jnp.float32
bf16 = jnp.bfloat16


def params(*semantics):
    return pltpu.CompilerParams(
        dimension_semantics=semantics or None, vmem_limit_bytes=VMEM
    )


def cost(flops, moved):
    return pl.CostEstimate(flops=int(flops), transcendentals=0, bytes_accessed=int(moved))


def normed_rows(values, gain):
    values = values.astype(f32)
    scaled = values * lax.rsqrt(jnp.mean(values * values, axis=-1, keepdims=True) + eps)
    return (scaled * gain).astype(bf16)


def head_pair(u, gain, cosine, sine):
    lane = lax.broadcasted_iota(jnp.int32, u.shape, 1)
    left = lane < HEAD
    square = u * u
    first = jnp.sum(jnp.where(left, square, 0.0), axis=-1, keepdims=True)
    second = jnp.sum(jnp.where(left, 0.0, square), axis=-1, keepdims=True)
    mean = jnp.where(left, first, second) * (1.0 / HEAD)
    u = u * lax.rsqrt(mean + eps) * gain
    half = HEAD // 2
    swapped = jnp.where(
        lane % HEAD < half, pltpu.roll(u, LANES - half, 1), pltpu.roll(u, half, 1)
    )
    return u * cosine + swapped * sine


def keyval_body(x_ref, gain_ref, kw_ref, vw_ref, kgain_ref, cos_ref, sin_ref, out_ref):
    normed = normed_rows(x_ref[...], gain_ref[...])
    keys = jnp.dot(normed, kw_ref[...], preferred_element_type=f32)
    values = jnp.dot(normed, vw_ref[...], preferred_element_type=f32)
    out_ref[:, :LANES] = head_pair(keys, kgain_ref[...], cos_ref[...], sin_ref[...]).astype(bf16)
    out_ref[:, LANES:] = values.astype(bf16)


def query_body(x_ref, gain_ref, qw_ref, qgain_ref, cos_ref, sin_ref, out_ref):
    normed = normed_rows(x_ref[...], gain_ref[...])
    rows = x_ref.shape[0]
    left = lax.broadcasted_iota(jnp.int32, (rows, LANES), 1) < HEAD
    scale = HEAD ** (-0.5)
    for pair in range(QHEADS // 2):
        u = jnp.dot(
            normed, qw_ref[:, pair * LANES : (pair + 1) * LANES], preferred_element_type=f32
        )
        u = head_pair(u, qgain_ref[...], cos_ref[...], sin_ref[...])
        u = u.astype(bf16).astype(f32) * scale
        moved = pltpu.roll(u, HEAD, 1)
        for odd in range(2):
            head = 2 * pair + odd
            group = head // (QHEADS // KVHEADS)
            source = u if odd == group else moved
            keep = left if group == 0 else jnp.logical_not(left)
            out_ref[head * rows : (head + 1) * rows, :] = jnp.where(keep, source, 0.0).astype(bf16)


def attend_body(q_ref, kv_ref, out_ref, peak_ref, acc_ref, *, own, group):
    step = pl.program_id(0)

    @pl.when(step == 0)
    def _():
        peak_ref[...] = jnp.full(peak_ref.shape, -jnp.inf, f32)
        acc_ref[...] = jnp.zeros(acc_ref.shape, f32)

    keys = kv_ref[:, :LANES]
    values = jnp.concatenate(
        [kv_ref[:, LANES:], jnp.ones((kv_ref.shape[0], LANES), bf16)], axis=1
    )

    def tile(start):
        rows = pl.ds(start, ROW_TILE)
        scores = lax.dot_general(
            q_ref[rows, :], keys, (((1,), (1,)), ((), ())), preferred_element_type=f32
        )
        before = peak_ref[rows, :1]
        fresh = jnp.maximum(before, jnp.max(scores, axis=-1, keepdims=True))
        factor = jnp.exp(before - fresh)
        weights = jnp.exp(scores - fresh).astype(bf16)
        peak_ref[rows, :] = jnp.broadcast_to(fresh, (ROW_TILE, LANES))
        acc_ref[rows, :] = acc_ref[rows, :] * factor + jnp.dot(
            weights, values, preferred_element_type=f32
        )

    def pair(index, carry):
        start = pl.multiple_of(index * (2 * ROW_TILE), 2 * ROW_TILE)
        tile(start)
        tile(start + ROW_TILE)
        return carry

    lax.fori_loop(0, q_ref.shape[0] // (2 * ROW_TILE), pair, 0)

    @pl.when(step == pl.num_programs(0) - 1)
    def _():
        left = lax.broadcasted_iota(jnp.int32, (own, LANES), 1) < HEAD
        for two in range(q_ref.shape[0] // (2 * own)):
            done = []
            for head in (2 * two, 2 * two + 1):
                block = acc_ref[head * own : (head + 1) * own, :]
                done.append(block[:, :LANES] / block[:, LANES:])
            if group == 0:
                both = jnp.where(left, done[0], pltpu.roll(done[1], HEAD, 1))
            else:
                both = jnp.where(left, pltpu.roll(done[0], HEAD, 1), done[1])
            out_ref[:, two * LANES : (two + 1) * LANES] = both.astype(bf16)


def attend(queries, keyvals, own, group):
    rows, keys = queries.shape[0] // KVHEADS, keyvals.shape[0]
    width = rows // own * HEAD
    return pl.pallas_call(
        functools.partial(attend_body, own=own, group=group),
        grid=(keys // KEY_BLOCK,),
        in_specs=[
            pl.BlockSpec((rows, LANES), lambda i: (group, 0)),
            pl.BlockSpec((KEY_BLOCK, 2 * LANES), lambda i: (i, 0)),
        ],
        out_specs=pl.BlockSpec((own, width), lambda i: (0, 0)),
        out_shape=jax.ShapeDtypeStruct((own, width), bf16),
        scratch_shapes=[
            pltpu.VMEM((rows, LANES), f32),
            pltpu.VMEM((rows, 2 * LANES), f32),
        ],
        compiler_params=params("arbitrary"),
        cost_estimate=cost(rows * keys * 1024, keys * 512),
        name="attend",
    )(queries, keyvals)


def route_body(x_ref, gain_ref, routes_ref, weights_ref, normed_ref, place_ref, spot_ref, share_ref):
    normed_ref[...] = normed_rows(x_ref[...], gain_ref[...])
    tokens, experts = spot_ref.shape
    expert = lax.broadcasted_iota(jnp.int32, (tokens, experts), 1)
    one = routes_ref[:, 0:1] == expert
    two = routes_ref[:, 1:2] == expert
    share_ref[...] = jnp.where(one, weights_ref[:, 0:1], 0.0) + jnp.where(
        two, weights_ref[:, 1:2], 0.0
    )
    named = jnp.where(jnp.logical_or(one, two), 1.0, 0.0)
    count = named.astype(bf16)
    row = lax.broadcasted_iota(jnp.int32, (tokens, tokens), 0)
    col = lax.broadcasted_iota(jnp.int32, (tokens, tokens), 1)
    earlier = jnp.where(col < row, 1.0, 0.0).astype(bf16)
    before = jnp.dot(earlier, count, preferred_element_type=f32)
    spot = jnp.where(named > 0.0, before, -1.0)
    spot_ref[...] = spot
    place_ref[...] = spot.T


def route(rows, gain, routes, weights, experts):
    tokens = rows.shape[0]
    return pl.pallas_call(
        route_body,
        out_shape=(
            jax.ShapeDtypeStruct((tokens, D), bf16),
            jax.ShapeDtypeStruct((experts, tokens), f32),
            jax.ShapeDtypeStruct((tokens, experts), f32),
            jax.ShapeDtypeStruct((tokens, experts), f32),
        ),
        compiler_params=params(),
        cost_estimate=cost(tokens * D * 100, tokens * D * 4),
        name="route",
    )(rows, gain, routes, weights)


def dispatch_body(place_ref, normed_ref, out_ref, pick_ref, *, which):
    experts, tokens = place_ref.shape
    owners = experts // EXP_DEV

    @pl.when(pl.program_id(0) == 0)
    def _():
        slot = lax.broadcasted_iota(jnp.int32, (CAP, tokens), 0).astype(f32)
        for owner in range(owners):
            expert = owner * EXP_DEV + which
            pick_ref[owner * CAP : (owner + 1) * CAP, :] = jnp.where(
                place_ref[expert : expert + 1, :] == slot, 1.0, 0.0
            ).astype(bf16)

    rows = jnp.dot(pick_ref[...], normed_ref[...], preferred_element_type=f32).astype(bf16)
    out_ref[...] = rows.reshape(out_ref.shape)


def dispatch(place, normed, which):
    experts, tokens = place.shape
    owners = experts // EXP_DEV
    block = 512
    return pl.pallas_call(
        functools.partial(dispatch_body, which=which),
        grid=(D // block,),
        in_specs=[
            pl.BlockSpec((experts, tokens), lambda i: (0, 0)),
            pl.BlockSpec((tokens, block), lambda i: (0, i)),
        ],
        out_specs=pl.BlockSpec((owners, CAP, block), lambda i: (0, 0, i)),
        out_shape=jax.ShapeDtypeStruct((owners, CAP, D), bf16),
        scratch_shapes=[pltpu.VMEM((owners * CAP, tokens), bf16)],
        compiler_params=params("arbitrary"),
        cost_estimate=cost(2 * owners * CAP * tokens * D, 6 * 2**20),
        name="dispatch",
    )(place, normed)


def expert_body(x_ref, gate_ref, up_ref, down_ref, out_ref):
    rows = x_ref[...].reshape(-1, D)
    gate = jnp.dot(rows, gate_ref[0], preferred_element_type=f32)
    upper = jnp.dot(rows, up_ref[0], preferred_element_type=f32)
    hidden = (gate * (1.0 / (1.0 + jnp.exp(-gate))) * upper).astype(bf16)
    out_ref[...] = (
        jnp.dot(hidden, down_ref[0], preferred_element_type=f32).astype(bf16).reshape(out_ref.shape)
    )


def expert(rows, gate, up, down, which):
    sources = rows.shape[0]
    tile = 4
    return pl.pallas_call(
        expert_body,
        grid=(sources // tile,),
        in_specs=[
            pl.BlockSpec((tile, CAP, D), lambda i: (i, 0, 0)),
            pl.BlockSpec((1, D, FF), lambda i: (which, 0, 0)),
            pl.BlockSpec((1, D, FF), lambda i: (which, 0, 0)),
            pl.BlockSpec((1, FF, D), lambda i: (which, 0, 0)),
        ],
        out_specs=pl.BlockSpec((tile, CAP, D), lambda i: (i, 0, 0)),
        out_shape=jax.ShapeDtypeStruct(rows.shape, bf16),
        compiler_params=params("arbitrary"),
        cost_estimate=cost(6 * sources * CAP * D * FF, 14 * 2**20),
        name="expert",
    )(rows, gate, up, down)


def combine_body(*refs, which, last):
    if last:
        spot_ref, share_ref, back_ref, part_ref, out_ref, high_ref, low_ref = refs
    else:
        spot_ref, share_ref, back_ref, out_ref, high_ref, low_ref = refs
    tokens, experts = spot_ref.shape

    @pl.when(pl.program_id(0) == 0)
    def _():
        lane = lax.broadcasted_iota(jnp.int32, (tokens, LANES), 1)
        left = lane < CAP
        slot = (lane % CAP).astype(f32)
        for two in range(experts // (2 * EXP_DEV)):
            near = 2 * two * EXP_DEV + which
            far = near + EXP_DEV
            spot = jnp.where(left, spot_ref[:, near : near + 1], spot_ref[:, far : far + 1])
            share = jnp.where(left, share_ref[:, near : near + 1], share_ref[:, far : far + 1])
            weight = jnp.where(spot == slot, share, 0.0)
            high = weight.astype(bf16)
            high_ref[:, two * LANES : (two + 1) * LANES] = high
            low_ref[:, two * LANES : (two + 1) * LANES] = (weight - high.astype(f32)).astype(bf16)

    back = back_ref[...].reshape(-1, back_ref.shape[-1])
    total = jnp.dot(high_ref[...], back, preferred_element_type=f32)
    total = total + jnp.dot(low_ref[...], back, preferred_element_type=f32)
    if last:
        total = total + part_ref[...]
    out_ref[...] = total.astype(out_ref.dtype)


def combine(spot, share, back, part, which):
    tokens, experts = spot.shape
    owners = experts // EXP_DEV
    last = part is not None
    block = 512
    small = pl.BlockSpec((tokens, experts), lambda i: (0, 0))
    column = pl.BlockSpec((tokens, block), lambda i: (0, i))
    specs = [small, small, pl.BlockSpec((owners, CAP, block), lambda i: (0, 0, i))]
    operands = [spot, share, back]
    if last:
        specs.append(column)
        operands.append(part)
    return pl.pallas_call(
        functools.partial(combine_body, which=which, last=last),
        grid=(D // block,),
        in_specs=specs,
        out_specs=column,
        out_shape=jax.ShapeDtypeStruct((tokens, D), bf16 if last else f32),
        scratch_shapes=[pltpu.VMEM((tokens, owners * CAP), bf16)] * 2,
        compiler_params=params("arbitrary"),
        cost_estimate=cost(4 * owners * CAP * tokens * D, 8 * 2**20),
        name="combine",
    )(*operands)


def tables(offset, count):
    lane = jnp.arange(LANES, dtype=jnp.int32)[None, :] + jnp.zeros((count, 1), jnp.int32)
    position = offset + jnp.arange(count, dtype=jnp.int32)[:, None] + jnp.zeros_like(lane)
    half = HEAD // 2
    freqs = half // 2
    inverse = theta ** (-((lane % freqs).astype(f32) * 2.0) / half)
    place = jnp.where(lane % half < freqs, position // GRID, position % GRID).astype(f32)
    angles = place * inverse
    sine = jnp.sin(angles)
    return jnp.cos(angles), jnp.where(lane % HEAD < half, -sine, sine)


def per_device(
    mixer_in,
    expert_in,
    mixer_gain,
    query_weight,
    key_weight,
    value_weight,
    query_gain,
    key_gain,
    output_weight,
    expert_gain,
    routes,
    route_weight,
    gate_weight,
    up_weight,
    down_weight,
):
    own = mixer_in.shape[0]
    offset = (lax.axis_index("ep") * lax.axis_size("tp") + lax.axis_index("tp")) * own
    cosine, sine = tables(offset, own)
    gain = mixer_gain.reshape(1, D)
    kgain = jnp.tile(key_gain, 2).reshape(1, LANES)
    qgain = jnp.tile(query_gain, 2).reshape(1, LANES)
    keyvals = pl.pallas_call(
        keyval_body,
        out_shape=jax.ShapeDtypeStruct((own, 2 * LANES), bf16),
        compiler_params=params(),
        cost_estimate=cost(own * D * 512, 2 * 2**20),
        name="keyval",
    )(mixer_in, gain, key_weight, value_weight, kgain, cosine, sine)
    everyone = lax.all_gather(keyvals, ("ep", "tp"), axis=0, tiled=True)

    experts = EXP_DEV * lax.axis_size("ep")
    normed, place, spot, share = route(
        expert_in, expert_gain.reshape(1, D), routes, route_weight, experts
    )

    def exchange(rows):
        return lax.all_to_all(rows, "ep", split_axis=0, concat_axis=0, tiled=True)

    arrived = [exchange(dispatch(place, normed, which)) for which in range(EXP_DEV)]
    queries = pl.pallas_call(
        query_body,
        out_shape=jax.ShapeDtypeStruct((QHEADS * own, LANES), bf16),
        compiler_params=params(),
        cost_estimate=cost(own * D * 2048, 5 * 2**20),
        name="query",
    )(mixer_in, gain, query_weight, qgain, cosine, sine)
    returned = []
    for which in range(EXP_DEV):
        result = expert(arrived[which], gate_weight, up_weight, down_weight, which)
        returned.append(exchange(result))
    pieces = []
    for group in range(KVHEADS):
        pieces.append(attend(queries, everyone, own, group))
    part = combine(spot, share, returned[0], None, 0)
    attended = jnp.concatenate(pieces, axis=1)
    mixer_out = jnp.dot(attended, output_weight, preferred_element_type=f32).astype(bf16)
    expert_out = combine(spot, share, returned[1], part, 1)
    return (mixer_out, expert_out)


def solution(mesh):
    placed = (
        P(("ep", "tp"), None),
        P(("ep", "tp"), None),
        P(),
        P(),
        P(),
        P(),
        P(),
        P(),
        P(),
        P(),
        P(("ep", "tp"), None),
        P(("ep", "tp"), None),
        P("ep", None, None),
        P("ep", None, None),
        P("ep", None, None),
    )

    return jax.shard_map(
        per_device,
        mesh=mesh,
        in_specs=placed,
        out_specs=(P(("ep", "tp"), None), P(("ep", "tp"), None)),
        check_vma=False,
    )
```

time: 606 us -> 392 us (0.65)
  matrix products: 159 us -> 2.42 us
  Pallas kernels: 0 us -> 143 us
  other arithmetic: 106 us -> 1.08 us
  local copies, waits for them, and re-layouts: 82.4 us -> 4.95 us
  blocking collectives: 55.4 us -> 0 us
  waiting for transfers between devices: 174 us -> 204 us
  starting transfers between devices: 13.2 us -> 21.8 us
    dot_general x22 -> x1, matrix products: 159 us -> 2.42 us  [per_device(): jnp.dot(attended, output_weight, preferred_element_type=f32).astype(bf16)]
    pallas_call x0 -> x11, Pallas kernels: none -> 143 us  [the longest x2 74.2 us: attend(): pl.pallas_call(functools.partial(attend_body, own=own, group=group), grid...]
    reduce_sum x12 -> x0, other arithmetic: 85.9 us -> none  [the longest x8 68.5 us: visit(): total = total * factor + jnp.sum(weights, axis=-1)]
    all_to_all x1 -> x0, blocking collectives: 55.4 us -> none  [cut_exchange(): lax.all_to_all(piece, axis, split_axis=0, concat_axis=0, tiled=True)]
    all_to_all x2 -> x4, waiting for transfers between devices: 174 us -> 204 us  [exchange(): return lax.all_to_all(rows, 'ep', split_axis=0, concat_axis=0, tiled=True)]
    gather x2 -> x0, local copies, waits for them, and re-layouts: 24.3 us -> none  [the longest x1 13.3 us: per_device(): returned.reshape(experts * capacity, D)[slot].reshape(token_rows, TOPK, D)]
    reshape x2 -> x0, local copies, waits for them, and re-layouts: 16.5 us -> none  [the longest x1 8.26 us: per_device(): blocks = piece.reshape(rows // span, span, 2 * width)]
    squeeze x8 -> x0, local copies, waits for them, and re-layouts: 10.4 us -> none  [per_device(): state, _ = lax.scan(visit, start_state, blocks)]
  transfers between devices with their start and end apart: 3 -> 5, of which waited for: 2 -> 4; matrix products, arithmetic and copies ran while one was open for 17% -> 1% of each run, Pallas kernels for 0% -> 17%
where the time goes in v1:
time: 392 us; the launch traced here: 391 us
  waiting for transfers between devices  204 us (52%)
  Pallas kernels  143 us (36%)
  starting transfers between devices  21.8 us (6%)
  between operations  14.1 us (4%)
  local copies, waits for them, and re-layouts  4.95 us (1%)
    all_to_all x4, waiting for transfers between devices, exchange(): return lax.all_to_all(rows, 'ep', split_axis=0, concat_axis=0, tiled=True)  204 us
    pallas_call x2, Pallas kernels, attend(): pl.pallas_call(functools.partial(attend_body, own=own, group=group), grid...  74.2 us
    pallas_call x2, Pallas kernels, expert(): pl.pallas_call(expert_body, grid=(sources // tile,), in_specs=[pl.BlockSp...  24.3 us
    all_to_all x4, starting transfers between devices, exchange(): return lax.all_to_all(rows, 'ep', split_axis=0, concat_axis=0, tiled=True)  21.8 us
    pallas_call x2, Pallas kernels, combine(): pl.pallas_call(functools.partial(combine_body, which=which, last=last), g...  20.7 us
    pallas_call x2, Pallas kernels, dispatch(): pl.pallas_call(functools.partial(dispatch_body, which=which), grid=(D //...  11.7 us
  transfers between devices with their start and end apart: 5, of which 4 were waited for; matrix products, arithmetic and copies ran while one was open for 1% of the time, Pallas kernels for 17%

profile of v1, /device:TPU:16, one launch (start us, length us, event | category | flops | bytes accessed | tf_op | source)
XLA Modules:
  0.0 391.1 jit_solution(15828996097358199843)
XLA Ops:
  7.3 0.7 tile.5
  8.6 1.0 negate_select_fusion
  9.6 2.6 keyval.1
  12.3 1.5 copy.17.routes_ref
  13.8 1.5 copy.18.weights_ref
  15.4 4.0 %route.1 = (bf16[512,2048]{1,0:T(8,128)(2,1)}, f32[32,512]{1,0:T(8,128)}, f32[512,32]{1,0:T(8,128)}, f32[512,32]{1,0:T(8,128)}) custom-call(bf16[512,2048]{1,0:T(8,128)(2,1)} %x_ref.5, f32[1,2048]{1,0:T(1,128)} %bitcast.5, s32[512,2]{1,0:T(8,128)} %copy.17.routes_ref, f32[512,2]{1,0:T(8,128)} %copy.18.weights_ref), custom_call_target="tpu_custom_call" | custom-call | flops 104857600 | bytes 4194304 | tf_op jit(solution)/shard_map/route/pallas_call | solution.py:184
  19.4 5.8 %dispatch.3 = bf16[16,64,2048]{2,1,0:T(8,128)(2,1)} custom-call(f32[32,512]{1,0:T(8,128)} %get-tuple-element.8.place_ref, bf16[512,2048]{1,0:T(8,128)(2,1)} %get-tuple-element.9.normed_ref), custom_call_target="tpu_custom_call" | custom-call | flops 2147483648 | bytes 6291456 | tf_op jit(solution)/shard_map/dispatch/pallas_call | solution.py:219
  25.2 7.9 %all-to-all-start.2 = ((bf16[16,64,2048]{2,1,0:T(8,128)(2,1)}), bf16[16,64,2048]{2,1,0:T(8,128)(2,1)}, u32[]{:S(2)}, u32[]{:S(2)}) async-start(bf16[16,64,2048]{2,1,0:T(8,128)(2,1)} %dispatch.3), calls=%async_computation.2 | async-start | bytes 8388608 | tf_op jit(solution)/shard_map/all_to_all | solution.py:370
  33.2 5.8 %dispatch.2 = bf16[16,64,2048]{2,1,0:T(8,128)(2,1)} custom-call(f32[32,512]{1,0:T(8,128)} %get-tuple-element.8.place_ref, bf16[512,2048]{1,0:T(8,128)(2,1)} %get-tuple-element.9.normed_ref), custom_call_target="tpu_custom_call" | custom-call | flops 2147483648 | bytes 6291456 | tf_op jit(solution)/shard_map/dispatch/pallas_call | solution.py:219
  39.0 59.0 %all-to-all-done.2.x_ref = bf16[16,64,2048]{2,1,0:T(8,128)(2,1)} async-done(((bf16[16,64,2048]{2,1,0:T(8,128)(2,1)}), bf16[16,64,2048]{2,1,0:T(8,128)(2,1)}, u32[]{:S(2)}, u32[]{:S(2)}) %all-to-all-start.2) | async-done | bytes 4194336 | tf_op jit(solution)/shard_map/all_to_all | solution.py:370
  98.0 4.6 %all-to-all-start = ((bf16[16,64,2048]{2,1,0:T(8,128)(2,1)}), bf16[16,64,2048]{2,1,0:T(8,128)(2,1)}, u32[]{:S(2)}, u32[]{:S(2)}) async-start(bf16[16,64,2048]{2,1,0:T(8,128)(2,1)} %dispatch.2), calls=%async_computation | async-start | bytes 8388608 | tf_op jit(solution)/shard_map/all_to_all | solution.py:370
  102.5 12.5 %expert.3 = bf16[16,64,2048]{2,1,0:T(8,128)(2,1)} custom-call(bf16[16,64,2048]{2,1,0:T(8,128)(2,1)} %all-to-all-done.2.x_ref, bf16[2,2048,512]{2,1,0:T(8,128)(2,1)} %gate_ref.3, bf16[2,2048,512]{2,1,0:T(8,128)(2,1)} %up_ref.3, bf16[2,512,2048]{2,1,0:T(8,128)(2,1)} %down_ref.3), custom_call_target="tpu_custom_call" | custom-call | flops 6442450944 | bytes 14680064 | tf_op jit(solution)/shard_map/expert/pallas_call | solution.py:248
  115.0 56.6 %all-to-all-done.x_ref = bf16[16,64,2048]{2,1,0:T(8,128)(2,1)} async-done(((bf16[16,64,2048]{2,1,0:T(8,128)(2,1)}), bf16[16,64,2048]{2,1,0:T(8,128)(2,1)}, u32[]{:S(2)}, u32[]{:S(2)}) %all-to-all-start) | async-done | bytes 4194336 | tf_op jit(solution)/shard_map/all_to_all | solution.py:370
  171.6 4.6 %all-to-all-start.3 = ((bf16[16,64,2048]{2,1,0:T(8,128)(2,1)}), bf16[16,64,2048]{2,1,0:T(8,128)(2,1)}, u32[]{:S(2)}, u32[]{:S(2)}) async-start(bf16[16,64,2048]{2,1,0:T(8,128)(2,1)} %expert.3), calls=%async_computation.3 | async-start | bytes 8388608 | tf_op jit(solution)/shard_map/all_to_all | solution.py:370
  176.2 11.8 %expert.2 = bf16[16,64,2048]{2,1,0:T(8,128)(2,1)} custom-call(bf16[16,64,2048]{2,1,0:T(8,128)(2,1)} %all-to-all-done.x_ref, bf16[2,2048,512]{2,1,0:T(8,128)(2,1)} %gate_ref.3, bf16[2,2048,512]{2,1,0:T(8,128)(2,1)} %up_ref.3, bf16[2,512,2048]{2,1,0:T(8,128)(2,1)} %down_ref.3), custom_call_target="tpu_custom_call" | custom-call | flops 6442450944 | bytes 14680064 | tf_op jit(solution)/shard_map/expert/pallas_call | solution.py:248
  187.9 47.9 %all-to-all-done.3.refs_2_ = bf16[16,64,2048]{2,1,0:T(8,128)(2,1)} async-done(((bf16[16,64,2048]{2,1,0:T(8,128)(2,1)}), bf16[16,64,2048]{2,1,0:T(8,128)(2,1)}, u32[]{:S(2)}, u32[]{:S(2)}) %all-to-all-start.3) | async-done | bytes 4194336 | tf_op jit(solution)/shard_map/all_to_all | solution.py:370
  235.8 4.7 %all-to-all-start.1 = ((bf16[16,64,2048]{2,1,0:T(8,128)(2,1)}), bf16[16,64,2048]{2,1,0:T(8,128)(2,1)}, u32[]{:S(2)}, u32[]{:S(2)}) async-start(bf16[16,64,2048]{2,1,0:T(8,128)(2,1)} %expert.2), calls=%async_computation.1 | async-start | bytes 8388608 | tf_op jit(solution)/shard_map/all_to_all | solution.py:370
  241.2 5.3 %query.1.q_ref = bf16[2048,128]{1,0:T(8,128)(2,1)} custom-call(bf16[128,2048]{1,0:T(8,128)(2,1)} %x_ref.4, f32[1,2048]{1,0:T(1,128)} %bitcast.4, bf16[2048,1024]{1,0:T(8,128)(2,1)} %qw_ref.1, f32[1,128]{1,0:T(1,128)} %reshape_tile.6.qgain_ref, f32[128,128]{1,0:T(8,128)} %get-tuple-element.11.cos_ref, f32[128,128]{1,0:T(8,128)} %get-tuple-element.10.sin_ref), custom_call_target="tpu_custom_call" | custom-call | flops 536870912 | bytes 5242880 | tf_op jit(solution)/shard_map/query/pallas_call | solution.py:373
  246.5 10.2 %combine.2.refs_3_ = f32[512,2048]{1,0:T(8,128)} custom-call(f32[512,32]{1,0:T(8,128)} %get-tuple-element.6.refs_0_, f32[512,32]{1,0:T(8,128)} %get-tuple-element.7.refs_1_, bf16[16,64,2048]{2,1,0:T(8,128)(2,1)} %all-to-all-done.3.refs_2_), custom_call_target="tpu_custom_call" | custom-call | flops 4294967296 | bytes 8388608 | tf_op jit(solution)/shard_map/combine/pallas_call | solution.py:307
  256.7 40.5 %all-to-all-done.1.refs_2_ = bf16[16,64,2048]{2,1,0:T(8,128)(2,1)} async-done(((bf16[16,64,2048]{2,1,0:T(8,128)(2,1)}), bf16[16,64,2048]{2,1,0:T(8,128)(2,1)}, u32[]{:S(2)}, u32[]{:S(2)}) %all-to-all-start.1) | async-done | bytes 4194336 | tf_op jit(solution)/shard_map/all_to_all | solution.py:370
  297.2 10.5 %combine.3 = bf16[512,2048]{1,0:T(8,128)(2,1)} custom-call(f32[512,32]{1,0:T(8,128)} %get-tuple-element.6.refs_0_, f32[512,32]{1,0:T(8,128)} %get-tuple-element.7.refs_1_, bf16[16,64,2048]{2,1,0:T(8,128)(2,1)} %all-to-all-done.1.refs_2_, f32[512,2048]{1,0:T(8,128)} %combine.2.refs_3_), custom_call_target="tpu_custom_call" | custom-call | flops 4294967296 | bytes 8388608 | tf_op jit(solution)/shard_map/combine/pallas_call | solution.py:307
  307.7 37.0 %attend.3 = bf16[128,512]{1,0:T(8,128)(2,1)} custom-call(bf16[2048,128]{1,0:T(8,128)(2,1)} %query.1.q_ref, bf16[16384,256]{1,0:T(8,128)(2,1)} %all-gather.2.cloned.1.call-done.kv_ref), custom_call_target="tpu_custom_call" | custom-call | flops 17179869184 | bytes 8388608 | tf_op jit(solution)/shard_map/attend/pallas_call | solution.py:143
  344.7 37.2 %attend.2 = bf16[128,512]{1,0:T(8,128)(2,1)} custom-call(bf16[2048,128]{1,0:T(8,128)(2,1)} %query.1.q_ref, bf16[16384,256]{1,0:T(8,128)(2,1)} %all-gather.2.cloned.1.call-done.kv_ref), custom_call_target="tpu_custom_call" | custom-call | flops 17179869184 | bytes 8388608 | tf_op jit(solution)/shard_map/attend/pallas_call | solution.py:143
  381.9 2.4 convolution_convert_fusion
  (20 shorter events, 1.3 us)
Async XLA Ops:
  7.2 300.5 %all-gather.2.cloned.1.call-start = ((), (), s32[]{:S(2)}) async-start(), calls=%async_computation.4 | async-start | bytes 8454144 | tf_op jit(solution)/shard_map/all_gather | solution.py:362
  25.2 72.7 %all-to-all-start.2 = ((bf16[16,64,2048]{2,1,0:T(8,128)(2,1)}), bf16[16,64,2048]{2,1,0:T(8,128)(2,1)}, u32[]{:S(2)}, u32[]{:S(2)}) async-start(bf16[16,64,2048]{2,1,0:T(8,128)(2,1)} %dispatch.3), calls=%async_computation.2 | async-start | bytes 8388608 | tf_op jit(solution)/shard_map/all_to_all | solution.py:370
  98.0 73.6 %all-to-all-start = ((bf16[16,64,2048]{2,1,0:T(8,128)(2,1)}), bf16[16,64,2048]{2,1,0:T(8,128)(2,1)}, u32[]{:S(2)}, u32[]{:S(2)}) async-start(bf16[16,64,2048]{2,1,0:T(8,128)(2,1)} %dispatch.2), calls=%async_computation | async-start | bytes 8388608 | tf_op jit(solution)/shard_map/all_to_all | solution.py:370
  171.6 64.2 %all-to-all-start.3 = ((bf16[16,64,2048]{2,1,0:T(8,128)(2,1)}), bf16[16,64,2048]{2,1,0:T(8,128)(2,1)}, u32[]{:S(2)}, u32[]{:S(2)}) async-start(bf16[16,64,2048]{2,1,0:T(8,128)(2,1)} %expert.3), calls=%async_computation.3 | async-start | bytes 8388608 | tf_op jit(solution)/shard_map/all_to_all | solution.py:370
  187.9 52.7 %copy-start.2 = (f32[64]{0:T(128)S(1)}, f32[64]{0:T(128)}, u32[]{:S(2)}) copy-start(f32[64]{0:T(128)} %param.21) | copy-start | bytes 772
  235.8 61.4 %all-to-all-start.1 = ((bf16[16,64,2048]{2,1,0:T(8,128)(2,1)}), bf16[16,64,2048]{2,1,0:T(8,128)(2,1)}, u32[]{:S(2)}, u32[]{:S(2)}) async-start(bf16[16,64,2048]{2,1,0:T(8,128)(2,1)} %expert.2), calls=%async_computation.1 | async-start | bytes 8388608 | tf_op jit(solution)/shard_map/all_to_all | solution.py:370
  344.7 37.2 %copy-start = (bf16[1024,2048]{1,0:T(8,128)(2,1)S(1)}, bf16[1024,2048]{1,0:T(8,128)(2,1)}, u32[]{:S(2)}) copy-start(bf16[1024,2048]{1,0:T(8,128)(2,1)} %param.23) | copy-start | bytes 12582916
  344.7 37.2 %copy-start.1 = (bf16[128,512]{1,0:T(8,128)(2,1)S(1)}, bf16[128,512]{1,0:T(8,128)(2,1)}, u32[]{:S(2)}) copy-start(bf16[128,512]{1,0:T(8,128)(2,1)} %attend.3) | copy-start | bytes 393220
Sparse Core Ops, SparseCore 0:
  12.4 149.7 all-gather.1

commit v2 on v1

v2 whole, which is shorter than its diff:
```python
import functools

import jax
import jax.numpy as jnp
from jax import lax
from jax.experimental import pallas as pl
from jax.experimental.pallas import tpu as pltpu
from jax.sharding import PartitionSpec as P


D = 2048
HEAD = 64
QHEADS = 16
KVHEADS = 2
GRID = 64
FF = 512
TOPK = 2
EXP_DEV = 2
CAP = 64
LANES = 128
KEY_BLOCK = 2048
ROW_TILE = 512
SIDE = 4
GROUPS = ((0, 10, 6, 14, 9, 11), (5, 15, 7, 13, 2, 8), (1, 3, 4, 12))
SAFE_LIMIT = 60.0
VMEM = 56 * 1024 * 1024

eps = 1e-06
theta = 10000.0
LOG2_E = 1.4426950408889634

f32 = jnp.float32
bf16 = jnp.bfloat16


def params(*semantics):
    return pltpu.CompilerParams(
        dimension_semantics=semantics or None, vmem_limit_bytes=VMEM
    )


def cost(flops, moved):
    return pl.CostEstimate(flops=int(flops), transcendentals=0, bytes_accessed=int(moved))


def normed_rows(values, gain):
    values = values.astype(f32)
    scaled = values * lax.rsqrt(jnp.mean(values * values, axis=-1, keepdims=True) + eps)
    return (scaled * gain).astype(bf16)


def head_pair(u, gain, cosine, sine):
    lane = lax.broadcasted_iota(jnp.int32, u.shape, 1)
    left = lane < HEAD
    square = u * u
    first = jnp.sum(jnp.where(left, square, 0.0), axis=-1, keepdims=True)
    second = jnp.sum(jnp.where(left, 0.0, square), axis=-1, keepdims=True)
    mean = jnp.where(left, first, second) * (1.0 / HEAD)
    u = u * lax.rsqrt(mean + eps) * gain
    half = HEAD // 2
    swapped = jnp.where(
        lane % HEAD < half, pltpu.roll(u, LANES - half, 1), pltpu.roll(u, half, 1)
    )
    return u * cosine + swapped * sine


def twice(gain):
    return jnp.concatenate([gain, gain], axis=1)


def keyval_body(x_ref, gain_ref, kw_ref, vw_ref, kgain_ref, cos_ref, sin_ref, out_ref):
    normed = normed_rows(x_ref[...], gain_ref[...])
    keys = jnp.dot(normed, kw_ref[...], preferred_element_type=f32)
    values = jnp.dot(normed, vw_ref[...], preferred_element_type=f32)
    out_ref[:, :LANES] = head_pair(keys, twice(kgain_ref[...]), cos_ref[...], sin_ref[...]).astype(bf16)
    out_ref[:, LANES:] = values.astype(bf16)


def query_body(x_ref, gain_ref, qw_ref, qgain_ref, cos_ref, sin_ref, out_ref):
    normed = normed_rows(x_ref[...], gain_ref[...])
    rows = x_ref.shape[0]
    left = lax.broadcasted_iota(jnp.int32, (rows, LANES), 1) < HEAD
    qgain = twice(qgain_ref[...])
    scale = HEAD ** (-0.5) * LOG2_E
    for pair in range(QHEADS // 2):
        u = jnp.dot(
            normed, qw_ref[:, pair * LANES : (pair + 1) * LANES], preferred_element_type=f32
        )
        u = head_pair(u, qgain, cos_ref[...], sin_ref[...])
        u = u.astype(bf16).astype(f32) * scale
        moved = pltpu.roll(u, HEAD, 1)
        for odd in range(2):
            head = 2 * pair + odd
            group = head // (QHEADS // KVHEADS)
            source = u if odd == group else moved
            keep = left if group == 0 else jnp.logical_not(left)
            source = jnp.where(keep, source, 0.0)
            high = source.astype(bf16)
            place = slice(head * rows, (head + 1) * rows)
            out_ref[place, :LANES] = high
            out_ref[place, LANES:] = (source - high.astype(f32)).astype(bf16)


def attend_body(safe_ref, q_ref, kv_ref, *refs, own, first, last):
    step = pl.program_id(0)
    if last:
        out_ref, peak_ref, acc_ref = refs[-3:]
    else:
        peak_ref, acc_ref = refs[-2:]

    @pl.when(step == 0)
    def _():
        if first:
            peak_ref[...] = jnp.full(peak_ref.shape, -jnp.inf, f32)
            acc_ref[...] = jnp.zeros(acc_ref.shape, f32)
        else:
            peak_ref[...] = refs[0][...]
            acc_ref[...] = refs[1][...]

    keys = kv_ref[:, :LANES]
    keys = jnp.concatenate([keys, keys], axis=1)
    values = kv_ref[:, LANES:]
    values = jnp.concatenate([values, jnp.ones(values.shape, bf16)], axis=1)

    def score(rows):
        return lax.dot_general(
            q_ref[rows, :], keys, (((1,), (1,)), ((), ())), preferred_element_type=f32
        )

    def gather(weights):
        return jnp.dot(weights.astype(bf16), values, preferred_element_type=f32)

    def plain(rows):
        acc_ref[rows, :] += gather(jnp.exp2(score(rows)))

    def careful(rows):
        scores = score(rows)
        before = peak_ref[rows, :1]
        fresh = jnp.maximum(before, jnp.max(scores, axis=-1, keepdims=True))
        peak_ref[rows, :] = jnp.broadcast_to(fresh, (fresh.shape[0], LANES))
        acc_ref[rows, :] = acc_ref[rows, :] * jnp.exp2(before - fresh) + gather(
            jnp.exp2(scores - fresh)
        )

    def sweep(work, tile, times):
        def some(index, carry):
            for time in range(times):
                start = pl.multiple_of((index * times + time) * tile, tile)
                work(pl.ds(start, tile))
            return carry

        lax.fori_loop(0, q_ref.shape[0] // (tile * times), some, 0)

    safe = safe_ref[0] <= SAFE_LIMIT

    @pl.when(safe)
    def _():
        sweep(plain, ROW_TILE, 2)

    @pl.when(jnp.logical_not(safe))
    def _():
        sweep(careful, ROW_TILE // 8, 1)

    if not last:
        return

    @pl.when(step == pl.num_programs(0) - 1)
    def _():
        left = lax.broadcasted_iota(jnp.int32, (own, LANES), 1) < HEAD
        for two in range(QHEADS // 2):
            done = []
            for head in (2 * two, 2 * two + 1):
                block = acc_ref[head * own : (head + 1) * own, :]
                done.append(block[:, :LANES] / block[:, LANES:])
            if 2 * two < QHEADS // KVHEADS:
                both = jnp.where(left, done[0], pltpu.roll(done[1], HEAD, 1))
            else:
                both = jnp.where(left, pltpu.roll(done[0], HEAD, 1), done[1])
            out_ref[:, two * LANES : (two + 1) * LANES] = both.astype(bf16)


def attend(safe, queries, keyvals, state, own, last):
    rows, keys = queries.shape[0], keyvals.shape[0]
    whole = lambda i: (0, 0)
    carried = [pl.BlockSpec((rows, LANES), whole), pl.BlockSpec((rows, 2 * LANES), whole)]
    shapes = [
        jax.ShapeDtypeStruct((rows, LANES), f32),
        jax.ShapeDtypeStruct((rows, 2 * LANES), f32),
    ]
    first = state is None
    return pl.pallas_call(
        functools.partial(attend_body, own=own, first=first, last=last),
        grid=(keys // KEY_BLOCK,),
        in_specs=[
            pl.BlockSpec(memory_space=pltpu.SMEM),
            pl.BlockSpec((rows, 2 * LANES), whole),
            pl.BlockSpec((KEY_BLOCK, 2 * LANES), lambda i: (i, 0)),
        ]
        + ([] if first else carried),
        out_specs=pl.BlockSpec((own, QHEADS * HEAD), whole) if last else carried,
        out_shape=jax.ShapeDtypeStruct((own, QHEADS * HEAD), bf16) if last else shapes,
        scratch_shapes=[pltpu.VMEM(shape.shape, f32) for shape in shapes] if last else [],
        compiler_params=params("arbitrary"),
        cost_estimate=cost(rows * keys * 1024, keys * 512),
        name="attend",
    )(safe, queries, keyvals, *([] if first else state))


def fill_pick(place_ref, pick_ref, group):
    slot = lax.broadcasted_iota(jnp.int32, (CAP, place_ref.shape[1]), 0).astype(f32)
    for index, shift in enumerate(group):
        for which in range(EXP_DEV):
            row = shift * EXP_DEV + which
            start = (index * EXP_DEV + which) * CAP
            pick_ref[start : start + CAP, :] = jnp.where(
                place_ref[row : row + 1, :] == slot, 1.0, 0.0
            ).astype(bf16)


def pick_rows(pick_ref, normed, out_refs):
    rows = jnp.dot(pick_ref[...], normed, preferred_element_type=f32).astype(bf16)
    span = EXP_DEV * CAP
    for index, out_ref in enumerate(out_refs):
        out_ref[...] = rows[index * span : (index + 1) * span].reshape(out_ref.shape)


def relative(routes, here_ref):
    holder = routes // EXP_DEV
    down = (holder // SIDE - here_ref[0] + SIDE) % SIDE
    across = (holder % SIDE - here_ref[1] + SIDE) % SIDE
    return (down * SIDE + across) * EXP_DEV + routes % EXP_DEV


def route_body(here_ref, x_ref, gain_ref, routes_ref, *refs, group):
    out_refs, (normed_ref, place_ref, named_ref, pick_ref) = refs[:-4], refs[-4:]
    step = pl.program_id(0)
    experts, tokens = place_ref.shape
    block = out_refs[0].shape[-1]

    @pl.when(step == 0)
    def _():
        named_ref[...] = relative(routes_ref[...], here_ref)
        expert = lax.broadcasted_iota(jnp.int32, (experts, tokens), 0)
        one = named_ref[0:1, :] == expert
        two = named_ref[1:2, :] == expert
        named = jnp.where(jnp.logical_or(one, two), 1.0, 0.0)
        row = lax.broadcasted_iota(jnp.int32, (tokens, tokens), 0)
        col = lax.broadcasted_iota(jnp.int32, (tokens, tokens), 1)
        earlier = jnp.where(row < col, 1.0, 0.0).astype(bf16)
        before = jnp.dot(named.astype(bf16), earlier, preferred_element_type=f32)
        place_ref[...] = jnp.where(named > 0.0, before, -1.0)
        fill_pick(place_ref, pick_ref, group)
        normed_ref[...] = normed_rows(x_ref[...], gain_ref[...])

    start = pl.multiple_of(step * block, block)
    pick_rows(pick_ref, normed_ref[:, pl.ds(start, block)], out_refs)


def bundles(count, block):
    return (
        [pl.BlockSpec((EXP_DEV, CAP, block), lambda i: (0, 0, i))] * count,
        [jax.ShapeDtypeStruct((EXP_DEV, CAP, D), bf16)] * count,
    )


def route(here, rows, gain, routes, experts, group):
    tokens = rows.shape[0]
    block = 512
    specs, shapes = bundles(len(group), block)
    whole = lambda i: (0, 0)
    return pl.pallas_call(
        functools.partial(route_body, group=group),
        grid=(D // block,),
        in_specs=[
            pl.BlockSpec(memory_space=pltpu.SMEM),
            pl.BlockSpec((tokens, D), whole),
            pl.BlockSpec((1, D), whole),
            pl.BlockSpec((TOPK, tokens), whole),
        ],
        out_specs=specs
        + [
            pl.BlockSpec((tokens, D), whole),
            pl.BlockSpec((experts, tokens), whole),
            pl.BlockSpec((TOPK, tokens), whole),
        ],
        out_shape=shapes
        + [
            jax.ShapeDtypeStruct((tokens, D), bf16),
            jax.ShapeDtypeStruct((experts, tokens), f32),
            jax.ShapeDtypeStruct((TOPK, tokens), jnp.int32),
        ],
        scratch_shapes=[pltpu.VMEM((len(group) * EXP_DEV * CAP, tokens), bf16)],
        compiler_params=params("arbitrary"),
        cost_estimate=cost(8e9, 8 * 2**20),
        name="route",
    )(here, rows, gain, routes)


def dispatch_body(place_ref, normed_ref, *refs, group):
    out_refs, pick_ref = refs[:-1], refs[-1]

    @pl.when(pl.program_id(0) == 0)
    def _():
        fill_pick(place_ref, pick_ref, group)

    pick_rows(pick_ref, normed_ref[...], out_refs)


def dispatch(place, normed, group):
    experts, tokens = place.shape
    block = 512
    specs, shapes = bundles(len(group), block)
    return pl.pallas_call(
        functools.partial(dispatch_body, group=group),
        grid=(D // block,),
        in_specs=[
            pl.BlockSpec((experts, tokens), lambda i: (0, 0)),
            pl.BlockSpec((tokens, block), lambda i: (0, i)),
        ],
        out_specs=specs,
        out_shape=shapes,
        scratch_shapes=[pltpu.VMEM((len(group) * EXP_DEV * CAP, tokens), bf16)],
        compiler_params=params("arbitrary"),
        cost_estimate=cost(5e9, 6 * 2**20),
        name="dispatch",
    )(place, normed)


def shares_body(place_ref, named_ref, weights_ref, *out_refs):
    experts, tokens = place_ref.shape
    expert = lax.broadcasted_iota(jnp.int32, (experts, tokens), 0)
    share = jnp.where(named_ref[0:1, :] == expert, weights_ref[0:1, :], 0.0) + jnp.where(
        named_ref[1:2, :] == expert, weights_ref[1:2, :], 0.0
    )
    slot = lax.broadcasted_iota(jnp.int32, (CAP, tokens), 0).astype(f32)
    for group, out_ref in zip(GROUPS, out_refs):
        for index, shift in enumerate(group):
            tiles = []
            for which in range(EXP_DEV):
                row = slice(shift * EXP_DEV + which, shift * EXP_DEV + which + 1)
                tiles.append(jnp.where(place_ref[row, :] == slot, share[row, :], 0.0))
            value = jnp.concatenate(tiles, axis=0).T
            high = value.astype(bf16)
            low = (value - high.astype(f32)).astype(bf16)
            columns = slice(index * LANES, (index + 1) * LANES)
            out_ref[:tokens, columns] = high
            out_ref[tokens:, columns] = low


def shares(place, named, weights):
    tokens = place.shape[1]
    return pl.pallas_call(
        shares_body,
        out_shape=[
            jax.ShapeDtypeStruct((2 * tokens, len(group) * LANES), bf16) for group in GROUPS
        ],
        compiler_params=params(),
        cost_estimate=cost(4e9, 4 * 2**20),
        name="shares",
    )(place, named, weights)


def expert_body(gate_ref, up_ref, down_ref, *refs):
    count = len(refs) // 2
    rows = jnp.concatenate([ref[0] for ref in refs[:count]], axis=0)
    gate = jnp.dot(rows, gate_ref[0], preferred_element_type=f32)
    upper = jnp.dot(rows, up_ref[0], preferred_element_type=f32)
    hidden = (gate * (1.0 / (1.0 + jnp.exp(-gate))) * upper).astype(bf16)
    result = jnp.dot(hidden, down_ref[0], preferred_element_type=f32).astype(bf16)
    for index, out_ref in enumerate(refs[count:]):
        out_ref[0] = result[index * CAP : (index + 1) * CAP]


def expert(arrays, gate, up, down):
    each = lambda i: (i, 0, 0)
    count = len(arrays)
    rows = [pl.BlockSpec((1, CAP, D), each)] * count
    return pl.pallas_call(
        expert_body,
        grid=(EXP_DEV,),
        in_specs=[
            pl.BlockSpec((1, D, FF), each),
            pl.BlockSpec((1, D, FF), each),
            pl.BlockSpec((1, FF, D), each),
        ]
        + rows,
        out_specs=rows,
        out_shape=[jax.ShapeDtypeStruct((EXP_DEV, CAP, D), bf16)] * count,
        compiler_params=params("arbitrary"),
        cost_estimate=cost(6 * count * EXP_DEV * CAP * D * FF, 14 * 2**20),
        name="expert",
    )(gate, up, down, *arrays)


def combine_body(share_ref, *refs, first):
    out_ref = refs[-1]
    back_refs = refs[:-1] if first else refs[:-2]
    tokens = out_ref.shape[0]
    back = jnp.concatenate([ref[...].reshape(-1, ref.shape[-1]) for ref in back_refs], axis=0)
    both = jnp.dot(share_ref[...], back, preferred_element_type=f32)
    total = both[:tokens] + both[tokens:]
    if not first:
        total = total + refs[-2][...]
    out_ref[...] = total.astype(out_ref.dtype)


def combine(share, arrays, part, last):
    tokens = share.shape[0] // 2
    block = 512
    column = pl.BlockSpec((tokens, block), lambda i: (0, i))
    specs = [pl.BlockSpec(share.shape, lambda i: (0, 0))] + bundles(len(arrays), block)[0]
    operands = [share, *arrays]
    if part is not None:
        specs.append(column)
        operands.append(part)
    return pl.pallas_call(
        functools.partial(combine_body, first=part is None),
        grid=(D // block,),
        in_specs=specs,
        out_specs=column,
        out_shape=jax.ShapeDtypeStruct((tokens, D), bf16 if last else f32),
        compiler_params=params("arbitrary"),
        cost_estimate=cost(4 * share.shape[1] * tokens * D, 8 * 2**20),
        name="combine",
    )(*operands)


def tables(offset, count):
    lane = jnp.arange(LANES, dtype=jnp.int32)[None, :] + jnp.zeros((count, 1), jnp.int32)
    position = offset + jnp.arange(count, dtype=jnp.int32)[:, None] + jnp.zeros_like(lane)
    half = HEAD // 2
    freqs = half // 2
    inverse = theta ** (-((lane % freqs).astype(f32) * 2.0) / half)
    place = jnp.where(lane % half < freqs, position // GRID, position % GRID).astype(f32)
    angles = place * inverse
    sine = jnp.sin(angles)
    return jnp.cos(angles), jnp.where(lane % HEAD < half, -sine, sine)


def per_device(
    mixer_in,
    expert_in,
    mixer_gain,
    query_weight,
    key_weight,
    value_weight,
    query_gain,
    key_gain,
    output_weight,
    expert_gain,
    routes,
    route_weight,
    gate_weight,
    up_weight,
    down_weight,
):
    own = mixer_in.shape[0]
    owners, sides = lax.axis_size("ep"), lax.axis_size("tp") // 2
    ep = lax.axis_index("ep")
    offset = (ep * lax.axis_size("tp") + lax.axis_index("tp")) * own
    here = jnp.stack([ep >> 2, ep & 3]).astype(jnp.int32)
    cosine, sine = tables(offset, own)
    gain = mixer_gain.reshape(1, D)
    bound = (
        1.02 * HEAD**0.5 * jnp.max(jnp.abs(query_gain)) * jnp.max(jnp.abs(key_gain))
    ).reshape(1)

    def shifted(array, shift, back=False):
        down, across = divmod(shift, SIDE)
        pairs = []
        for z in range(SIDE):
            for x in range(SIDE):
                pair = (z * SIDE + x, (z + down) % SIDE * SIDE + (x + across) % SIDE)
                pairs.append(pair[::-1] if back else pair)
        return lax.ppermute(array, "ep", pairs)

    keyvals = pl.pallas_call(
        keyval_body,
        out_shape=jax.ShapeDtypeStruct((own, 2 * LANES), bf16),
        compiler_params=params(),
        cost_estimate=cost(own * D * 512, 2 * 2**20),
        name="keyval",
    )(mixer_in, gain, key_weight, value_weight, key_gain.reshape(1, HEAD), cosine, sine)
    line = jnp.concatenate(
        [keyvals] + [shifted(keyvals, SIDE * turn) for turn in range(1, SIDE)], axis=0
    )
    plane = jnp.concatenate([line] + [shifted(line, turn) for turn in range(1, SIDE)], axis=0)
    near = [plane]
    for turn in range(1, sides):
        ring = [(2 * y + c, 2 * ((y + turn) % sides) + c) for y in range(sides) for c in range(2)]
        near.append(lax.ppermute(plane, "tp", ring))
    near = jnp.concatenate(near, axis=0)
    far = lax.ppermute(near, "tp", [(i, i ^ 1) for i in range(2 * sides)])

    *first, normed, place, named = route(
        here,
        expert_in,
        expert_gain.reshape(1, D),
        routes.T,
        EXP_DEV * owners,
        GROUPS[0],
    )
    outgoing = dict(zip(GROUPS[0], first))
    rest = sum(GROUPS[1:], ())
    outgoing.update(zip(rest, dispatch(place, normed, rest)))
    queries = pl.pallas_call(
        query_body,
        out_shape=jax.ShapeDtypeStruct((QHEADS * own, 2 * LANES), bf16),
        compiler_params=params(),
        cost_estimate=cost(own * D * 2048, 5 * 2**20),
        name="query",
    )(mixer_in, gain, query_weight, query_gain.reshape(1, HEAD), cosine, sine)
    share = shares(place, named, route_weight.T)

    returned = {}
    for group in GROUPS:
        arrived = [
            shifted(array, shift) if shift else array
            for shift in group
            for array in (outgoing[shift],)
        ]
        results = expert(arrived, gate_weight, up_weight, down_weight)
        for shift, array in zip(group, results):
            returned[shift] = shifted(array, shift, True) if shift else array
    state = attend(bound, queries, near, None, own, False)
    attended = attend(bound, queries, far, state, own, True)
    mixer_out = jnp.dot(attended, output_weight, preferred_element_type=f32).astype(bf16)
    total = None
    for number, group in enumerate(GROUPS):
        arrays = [returned[shift] for shift in group]
        total = combine(share[number], arrays, total, number == len(GROUPS) - 1)
    return (mixer_out, total)


def solution(mesh):
    placed = (
        P(("ep", "tp"), None),
        P(("ep", "tp"), None),
        P(),
        P(),
        P(),
        P(),
        P(),
        P(),
        P(),
        P(),
        P(("ep", "tp"), None),
        P(("ep", "tp"), None),
        P("ep", None, None),
        P("ep", None, None),
        P("ep", None, None),
    )

    return jax.shard_map(
        per_device,
        mesh=mesh,
        in_specs=placed,
        out_specs=(P(("ep", "tp"), None), P(("ep", "tp"), None)),
        check_vma=False,
    )
```

time: 392 us -> 603 us (1.54)
  the two profiles are of different devices: /device:TPU:16 before, /device:TPU:64 now
where the time goes in v2:
time: 603 us; the launch traced here: 602 us
  Pallas kernels  369 us (61%)
  waiting for transfers between devices  132 us (22%)
  starting transfers between devices  81.4 us (13%)
  local copies, waits for them, and re-layouts  11.6 us (2%)
    pallas_call x2, Pallas kernels, attend(): pl.pallas_call(functools.partial(attend_body, own=own, first=first, last=...  295 us
    ppermute x36, waiting for transfers between devices, shifted(): return lax.ppermute(array, 'ep', pairs)  132 us
    ppermute x36, starting transfers between devices, shifted(): return lax.ppermute(array, 'ep', pairs)  72.3 us
    pallas_call x3, Pallas kernels, expert(): pl.pallas_call(expert_body, grid=(EXP_DEV,), in_specs=[pl.BlockSpec((1, D...  27.4 us
    pallas_call x3, Pallas kernels, combine(): pl.pallas_call(functools.partial(combine_body, first=part is None), grid=...  22.4 us
  transfers between devices with their start and end apart: 40, of which 13 were waited for; matrix products, arithmetic and copies ran while one was open for 2% of the time, Pallas kernels for 36%

profile of v2, /device:TPU:64, one launch (start us, length us, event | category | flops | bytes accessed | tf_op | source)
XLA Modules:
  0.0 602.3 jit_solution(4686381668338840990)
XLA Ops:
  8.1 6.7 %route.1 = (bf16[2,64,2048]{2,1,0:T(8,128)(2,1)}, bf16[2,64,2048]{2,1,0:T(8,128)(2,1)}, bf16[2,64,2048]{2,1,0:T(8,128)(2,1)}, bf16[2,64,2048]{2,1,0:T(8,128)(2,1...) custom-call(s32[2]{0:T(128)} %pad_add_fusion.here_ref, ...), custom_call_target="tpu_custom_call" | custom-call | flops 8000000000 | bytes 8388608 | tf_op jit(solution)/shard_map/route/pallas_call | solution.py:271
  14.8 5.6 collective-permute-start.30
  30.2 20.4 %collective-permute-done.3 = bf16[512,256]{1,0:T(8,128)(2,1)S(1)} collective-permute-done((bf16[512,256]{1,0:T(8,128)(2,1)S(1)}, bf16[512,256]{1,0:T(8,128)(2,1)S(1)}, u32[]{:S(2)}, u32[]{:S(2)}) %collective-permute-start.3) | collective-permute-done | bytes 262176 | tf_op jit(solution)/shard_map/ppermute | solution.py:475
  61.8 6.3 %dispatch.1 = (bf16[2,64,2048]{2,1,0:T(8,128)(2,1)}, bf16[2,64,2048]{2,1,0:T(8,128)(2,1)}, bf16[2,64,2048]{2,1,0:T(8,128)(2,1)}, bf16[2,64,2048]{2,1,0:T(8,128)(...) custom-call(f32[32,512]{1,0:T(8,128)} %get-tuple-element.44.place_re, ...), custom_call_target="tpu_custom_call" | custom-call | flops 5000000000 | bytes 6291456 | tf_op jit(solution)/shard_map/dispatch/pallas_call | solution.py:313
  68.2 5.6 collective-permute-start.34
  74.2 13.8 %collective-permute-done.33.refs_4_ = bf16[2,64,2048]{2,1,0:T(8,128)(2,1)S(1)} collective-permute-done((bf16[2,64,2048]{2,1,0:T(8,128)(2,1)}, bf16[2,64,2048]{2,1,0:T(8,128)(2,1)S(1)}, u32[]{:S(2)}, u32[]{:S(2)}) %collective-permute-start.33) | collective-permute-done | bytes 524320 | tf_op jit(solution)/shard_map/ppermute | solution.py:475
  92.5 9.9 %collective-permute-done.34.refs_5_ = bf16[2,64,2048]{2,1,0:T(8,128)(2,1)S(1)} collective-permute-done((bf16[2,64,2048]{2,1,0:T(8,128)(2,1)S(1)}, bf16[2,64,2048]{2,1,0:T(8,128)(2,1)S(1)}, u32[]{:S(2)}, u32[]{:S(2)}) %collective-permute-start.34) | collective-permute-done | bytes 524320 | tf_op jit(solution)/shard_map/ppermute | solution.py:475
  110.5 10.9 %collective-permute-done.19.refs_1_ = bf16[2,64,2048]{2,1,0:T(8,128)(2,1)S(1)} collective-permute-done((bf16[2,64,2048]{2,1,0:T(8,128)(2,1)}, bf16[2,64,2048]{2,1,0:T(8,128)(2,1)S(1)}, u32[]{:S(2)}, u32[]{:S(2)}) %collective-permute-start.19) | collective-permute-done | bytes 524320 | tf_op jit(solution)/shard_map/ppermute | solution.py:475
  124.8 14.3 %collective-permute-done.20.refs_2_ = bf16[2,64,2048]{2,1,0:T(8,128)(2,1)S(1)} collective-permute-done((bf16[2,64,2048]{2,1,0:T(8,128)(2,1)}, bf16[2,64,2048]{2,1,0:T(8,128)(2,1)S(1)}, u32[]{:S(2)}, u32[]{:S(2)}) %collective-permute-start.20) | collective-permute-done | bytes 524320 | tf_op jit(solution)/shard_map/ppermute | solution.py:475
  144.3 9.7 %expert.5 = (bf16[2,64,2048]{2,1,0:T(8,128)(2,1)}, bf16[2,64,2048]{2,1,0:T(8,128)(2,1)}, bf16[2,64,2048]{2,1,0:T(8,128)(2,1)}, bf16[2,64,2048]{2,1,0:T(8,128)(2,...) custom-call(bf16[2,2048,512]{2,1,0:T(8,128)(2,1)} %gate_ref.5, bf16[2,2048,512]{2,1,0:T(8,128)(2,1)} %up_ref.5, ...), custom_call_target="tpu_custom_call" | custom-call | flops 4831838208 | bytes 14680064 | tf_op jit(solution)/shard_map/expert/pallas_call | solution.py:378
  164.4 9.7 %expert.4 = (bf16[2,64,2048]{2,1,0:T(8,128)(2,1)}, bf16[2,64,2048]{2,1,0:T(8,128)(2,1)}, bf16[2,64,2048]{2,1,0:T(8,128)(2,1)}, bf16[2,64,2048]{2,1,0:T(8,128)(2,...) custom-call(bf16[2,2048,512]{2,1,0:T(8,128)(2,1)} %gate_ref.5, bf16[2,2048,512]{2,1,0:T(8,128)(2,1)} %up_ref.5, ...), custom_call_target="tpu_custom_call" | custom-call | flops 4831838208 | bytes 14680064 | tf_op jit(solution)/shard_map/expert/pallas_call | solution.py:378
  174.1 16.7 %collective-permute-done.13.refs_3_ = bf16[2,64,2048]{2,1,0:T(8,128)(2,1)S(1)} collective-permute-done((bf16[2,64,2048]{2,1,0:T(8,128)(2,1)S(1)}, bf16[2,64,2048]{2,1,0:T(8,128)(2,1)S(1)}, u32[]{:S(2)}, u32[]{:S(2)}) %collective-permute-start.13) | collective-permute-done | bytes 524320 | tf_op jit(solution)/shard_map/ppermute | solution.py:475
  190.8 7.8 %collective-permute-start.38 = (bf16[2,64,2048]{2,1,0:T(8,128)(2,1)}, bf16[2,64,2048]{2,1,0:T(8,128)(2,1)}, u32[]{:S(2)}, u32[]{:S(2)}) collective-permute-start(bf16[2,64,2048]{2,1,0:T(8,128)(2,1)} %get-tuple-element.80), channel_id=1, source_target_pairs={{72,0},{80,8},{88,16},{64,24},{104,32},{112,40},{120,48},{96,56},{... | collective-permute-start | bytes 1572872 | tf_op jit(solution)/shard_map/ppermute | solution.py:475
  198.6 6.4 %collective-permute-start.24 = (bf16[2,64,2048]{2,1,0:T(8,128)(2,1)}, bf16[2,64,2048]{2,1,0:T(8,128)(2,1)S(1)}, u32[]{:S(2)}, u32[]{:S(2)}) collective-permute-start(bf16[2,64,2048]{2,1,0:T(8,128)(2,1)} %get-tuple-element.63), channel_id=1, source_target_pairs={{40,0},{48,8},{56,16},{32,24},{72,32},{80,40},{88,48},{64,56},{104... | collective-permute-start | bytes 1572872 | tf_op jit(solution)/shard_map/ppermute | solution.py:475
  207.7 5.9 query.1.q_ref
  213.5 12.8 %collective-permute-done.38.refs_4_ = bf16[2,64,2048]{2,1,0:T(8,128)(2,1)} collective-permute-done((bf16[2,64,2048]{2,1,0:T(8,128)(2,1)}, bf16[2,64,2048]{2,1,0:T(8,128)(2,1)}, u32[]{:S(2)}, u32[]{:S(2)}) %collective-permute-start.38) | collective-permute-done | bytes 524320 | tf_op jit(solution)/shard_map/ppermute | solution.py:475
  230.5 6.0 collective-permute-done.24.refs_0_
  246.3 8.0 %expert.3 = (bf16[2,64,2048]{2,1,0:T(8,128)(2,1)}, bf16[2,64,2048]{2,1,0:T(8,128)(2,1)}, bf16[2,64,2048]{2,1,0:T(8,128)(2,1)}, bf16[2,64,2048]{2,1,0:T(8,128)(2,1)}) custom-call(bf16[2,2048,512]{2,1,0:T(8,128)(2,1)} %gate_ref.5, bf16[2,2048,512]{2,1,0:T(8,128)(2,1)} %up_ref.5, bf16[2,512,2048]{2,1,0:T(8,128)(2,1)} %down_ref.5, ...), custom_call_target="tpu_custom_call" | custom-call | flops 3221225472 | bytes 14680064 | tf_op jit(solution)/shard_map/expert/pallas_call | solution.py:378
  259.4 20.1 %collective-permute-done.28.refs_4_ = bf16[2,64,2048]{2,1,0:T(8,128)(2,1)S(1)} collective-permute-done((bf16[2,64,2048]{2,1,0:T(8,128)(2,1)S(1)}, bf16[2,64,2048]{2,1,0:T(8,128)(2,1)S(1)}, u32[]{:S(2)}, u32[]{:S(2)}) %collective-permute-start.28) | collective-permute-done | bytes 524320 | tf_op jit(solution)/shard_map/ppermute | solution.py:475
  281.5 7.5 %combine.3.refs_6_ = f32[512,2048]{1,0:T(8,128)} custom-call(bf16[1024,768]{1,0:T(8,128)(2,1)} %get-tuple-element.69.share_ref, bf16[2,64,2048]{2,1,0:T(8,128)(2,1)} %get-tuple-element.76.refs_0_, bf16[2,64,2048]{2,1,0:T(8,128)(2,1)} %copy-done.22, bf16[2,64,2048]{2,1,0:T(8,128)(2,1)} %copy-done.23, bf16[2,64,2048]{2,1,0:T(8,128)(2,1)} %copy-done.26, ...), custom_call_target="tpu_custom_call" | custom-call | flops 3221225472 | bytes 8388608 | tf_op jit(solution)/shard_map/combine/pallas_call | solution.py:416
  289.0 8.3 %combine.4.refs_4_ = f32[512,2048]{1,0:T(8,128)} custom-call(bf16[1024,768]{1,0:T(8,128)(2,1)} %get-tuple-element.56.share_ref, bf16[2,64,2048]{2,1,0:T(8,128)(2,1)} %copy-done.6, bf16[2,64,2048]{2,1,0:T(8,128)(2,1)} %copy-done.7, bf16[2,64,2048]{2,1,0:T(8,128)(2,1)} %copy-done.8, bf16[2,64,2048]{2,1,0:T(8,128)(2,1)} %copy-done.9, ...), custom_call_target="tpu_custom_call" | custom-call | flops 3221225472 | bytes 8388608 | tf_op jit(solution)/shard_map/combine/pallas_call | solution.py:416
  298.6 6.6 %combine.5 = bf16[512,2048]{1,0:T(8,128)(2,1)} custom-call(bf16[1024,512]{1,0:T(8,128)(2,1)} %get-tuple-element.46.share_ref, bf16[2,64,2048]{2,1,0:T(8,128)(2,1)} %copy-done.12, bf16[2,64,2048]{2,1,0:T(8,128)(2,1)} %copy-done.13, bf16[2,64,2048]{2,1,0:T(8,128)(2,1)} %copy-done.14, bf16[2,64,2048]{2,1,0:T(8,128)(2,1)} %copy-done.15, f32[512,2048]{1,0:T(8,128)} %combine.4.refs_4_), custom_call_target="tpu_custom_call" | custom-call | flops 2147483648 | bytes 8388608 | tf_op jit(solution)/shard_map/combine/pallas_call | solution.py:416
  305.2 147.1 %attend.2 = (f32[2048,128]{1,0:T(8,128)}, f32[2048,256]{1,0:T(8,128)}) custom-call(f32[1]{0:T(128)} %bitcast.safe_ref, bf16[2048,256]{1,0:T(8,128)(2,1)} %query.1.q_ref, bf16[8192,256]{1,0:T(8,128)(2,1)} %constant_dynamic-update-slice_fusion.7.kv_ref), custom_call_target="tpu_custom_call" | custom-call | flops 17179869184 | bytes 4194304 | tf_op jit(solution)/shard_map/attend/pallas_call | solution.py:191
  452.3 147.5 %attend.3 = bf16[128,1024]{1,0:T(8,128)(2,1)} custom-call(f32[1]{0:T(128)} %bitcast.safe_ref, bf16[2048,256]{1,0:T(8,128)(2,1)} %query.1.q_ref, bf16[8192,256]{1,0:T(8,128)(2,1)} %collective-permute-done.9.kv_ref, f32[2048,128]{1,0:T(8,128)} %get-tuple-element.42.refs_0_, f32[2048,256]{1,0:T(8,128)} %get-tuple-element.43.refs_1_), custom_call_target="tpu_custom_call" | custom-call | flops 17179869184 | bytes 4194304 | tf_op jit(solution)/shard_map/attend/pallas_call | solution.py:191
  (175 shorter events, 86.4 us)
Async XLA Ops:
  14.8 44.0 %collective-permute-start.30 = (bf16[2,64,2048]{2,1,0:T(8,128)(2,1)}, bf16[2,64,2048]{2,1,0:T(8,128)(2,1)S(1)}, u32[]{:S(2)}, u32[]{:S(2)}) collective-permute-start(bf16[2,64,2048]{2,1,0:T(8,128)(2,1)} %get-tuple-element.71), channel_id=1, source_target_pairs={{0,80},{8,88},{16,64},{24,72},{32,112},{40,120},{48,96},{56,104},{... | collective-permute-start | bytes 1572872 | tf_op jit(solution)/shard_map/ppermute | solution.py:475
  20.4 47.8 %collective-permute-start.31 = (bf16[2,64,2048]{2,1,0:T(8,128)(2,1)}, bf16[2,64,2048]{2,1,0:T(8,128)(2,1)S(1)}, u32[]{:S(2)}, u32[]{:S(2)}) collective-permute-start(bf16[2,64,2048]{2,1,0:T(8,128)(2,1)} %get-tuple-element.72), channel_id=1, source_target_pairs={{0,48},{8,56},{16,32},{24,40},{32,80},{40,88},{48,64},{56,72},{64,... | collective-permute-start | bytes 1572872 | tf_op jit(solution)/shard_map/ppermute | solution.py:475
  24.2 30.9 %collective-permute-start.4 = (bf16[512,256]{1,0:T(8,128)(2,1)S(1)}, bf16[512,256]{1,0:T(8,128)(2,1)S(1)}, u32[]{:S(2)}, u32[]{:S(2)}) collective-permute-start(bf16[512,256]{1,0:T(8,128)(2,1)S(1)} %pad_maximum_fusion), channel_id=1, source_target_pairs={{0,16},{8,24},{16,0},{24,8},{32,48},{40,56},{48,32},{56,40},{64,80... | collective-permute-start | bytes 786440 | tf_op jit(solution)/shard_map/ppermute | solution.py:475
  57.2 45.9 %collective-permute-start.6 = (bf16[2048,256]{1,0:T(8,128)(2,1)S(1)}, bf16[2048,256]{1,0:T(8,128)(2,1)S(1)}, u32[]{:S(2)}, u32[]{:S(2)}) collective-permute-start(bf16[2048,256]{1,0:T(8,128)(2,1)S(1)} %get-tuple-element.82), channel_id=1, source_target_pairs={{0,2},{1,3},{2,4},{3,5},{4,6},{5,7},{6,0},{7,1},{8,10},{9,11},{10,... | collective-permute-start | bytes 3145736 | tf_op jit(solution)/shard_map/ppermute | solution.py:491
  58.8 48.6 %collective-permute-start.7 = (bf16[2048,256]{1,0:T(8,128)(2,1)S(1)}, bf16[2048,256]{1,0:T(8,128)(2,1)S(1)}, u32[]{:S(2)}, u32[]{:S(2)}) collective-permute-start(bf16[2048,256]{1,0:T(8,128)(2,1)S(1)} %get-tuple-element.82), channel_id=1, source_target_pairs={{0,4},{1,5},{2,6},{3,7},{4,0},{5,1},{6,2},{7,3},{8,12},{9,13},{10,... | collective-permute-start | bytes 3145736 | tf_op jit(solution)/shard_map/ppermute | solution.py:491
  68.2 34.2 %collective-permute-start.34 = (bf16[2,64,2048]{2,1,0:T(8,128)(2,1)S(1)}, bf16[2,64,2048]{2,1,0:T(8,128)(2,1)S(1)}, u32[]{:S(2)}, u32[]{:S(2)}) collective-permute-start(bf16[2,64,2048]{2,1,0:T(8,128)(2,1)S(1)} %copy-done.24), channel_id=1, source_target_pairs={{0,88},{8,64},{16,72},{24,80},{32,120},{40,96},{48,104},{56,112},{... | collective-permute-start | bytes 1572872 | tf_op jit(solution)/shard_map/ppermute | solution.py:475
  88.0 54.4 %collective-permute-start.8 = (bf16[2048,256]{1,0:T(8,128)(2,1)S(1)}, bf16[2048,256]{1,0:T(8,128)(2,1)S(1)}, u32[]{:S(2)}, u32[]{:S(2)}) collective-permute-start(bf16[2048,256]{1,0:T(8,128)(2,1)S(1)} %get-tuple-element.82), channel_id=1, source_target_pairs={{0,6},{1,7},{2,0},{3,1},{4,2},{5,3},{6,4},{7,5},{8,14},{9,15},{10,... | collective-permute-start | bytes 3145736 | tf_op jit(solution)/shard_map/ppermute | solution.py:491
  103.2 35.9 %collective-permute-start.20 = (bf16[2,64,2048]{2,1,0:T(8,128)(2,1)}, bf16[2,64,2048]{2,1,0:T(8,128)(2,1)S(1)}, u32[]{:S(2)}, u32[]{:S(2)}) collective-permute-start(bf16[2,64,2048]{2,1,0:T(8,128)(2,1)} %get-tuple-element.59), channel_id=1, source_target_pairs={{0,56},{8,32},{16,40},{24,48},{32,88},{40,64},{48,72},{56,80},{64,... | collective-permute-start | bytes 1572872 | tf_op jit(solution)/shard_map/ppermute | solution.py:475
  103.2 35.9 %collective-permute-start.21 = (bf16[2,64,2048]{2,1,0:T(8,128)(2,1)}, bf16[2,64,2048]{2,1,0:T(8,128)(2,1)S(1)}, u32[]{:S(2)}, u32[]{:S(2)}) collective-permute-start(bf16[2,64,2048]{2,1,0:T(8,128)(2,1)} %get-tuple-element.60), channel_id=1, source_target_pairs={{0,104},{8,112},{16,120},{24,96},{32,8},{40,16},{48,24},{56,0},{64... | collective-permute-start | bytes 1572872 | tf_op jit(solution)/shard_map/ppermute | solution.py:475
  107.4 36.0 %collective-permute-start.22 = (bf16[2,64,2048]{2,1,0:T(8,128)(2,1)}, bf16[2,64,2048]{2,1,0:T(8,128)(2,1)S(1)}, u32[]{:S(2)}, u32[]{:S(2)}) collective-permute-start(bf16[2,64,2048]{2,1,0:T(8,128)(2,1)} %get-tuple-element.61), channel_id=1, source_target_pairs={{0,16},{8,24},{16,0},{24,8},{32,48},{40,56},{48,32},{56,40},{64,80... | collective-permute-start | bytes 1572872 | tf_op jit(solution)/shard_map/ppermute | solution.py:475
  121.4 32.7 %collective-permute-start.23 = (bf16[2,64,2048]{2,1,0:T(8,128)(2,1)}, bf16[2,64,2048]{2,1,0:T(8,128)(2,1)S(1)}, u32[]{:S(2)}, u32[]{:S(2)}) collective-permute-start(bf16[2,64,2048]{2,1,0:T(8,128)(2,1)} %get-tuple-element.62), channel_id=1, source_target_pairs={{0,64},{8,72},{16,80},{24,88},{32,96},{40,104},{48,112},{56,120},{... | collective-permute-start | bytes 1572872 | tf_op jit(solution)/shard_map/ppermute | solution.py:475
  143.5 308.9 %collective-permute-start.9 = (bf16[8192,256]{1,0:T(8,128)(2,1)}, bf16[8192,256]{1,0:T(8,128)(2,1)}, u32[]{:S(2)}, u32[]{:S(2)}) collective-permute-start(bf16[8192,256]{1,0:T(8,128)(2,1)} %constant_dynamic-update-slice_fusion.7.kv_ref), channel_id=1, source_target_pairs={{0,1},{1,0},{2,3},{3,2},{4,5},{5,4},{6,7},{7,6},{8,9},{9,8},{10,11... | collective-permute-start | bytes 12582920 | tf_op jit(solution)/shard_map/ppermute | solution.py:493
  154.8 36.0 %collective-permute-start.13 = (bf16[2,64,2048]{2,1,0:T(8,128)(2,1)S(1)}, bf16[2,64,2048]{2,1,0:T(8,128)(2,1)S(1)}, u32[]{:S(2)}, u32[]{:S(2)}) collective-permute-start(bf16[2,64,2048]{2,1,0:T(8,128)(2,1)S(1)} %copy-done.21), channel_id=1, source_target_pairs={{0,96},{8,104},{16,112},{24,120},{32,0},{40,8},{48,16},{56,24},{64... | collective-permute-start | bytes 1572872 | tf_op jit(solution)/shard_map/ppermute | solution.py:475
  156.9 41.7 %collective-permute-start.35 = (bf16[2,64,2048]{2,1,0:T(8,128)(2,1)}, bf16[2,64,2048]{2,1,0:T(8,128)(2,1)S(1)}, u32[]{:S(2)}, u32[]{:S(2)}) collective-permute-start(bf16[2,64,2048]{2,1,0:T(8,128)(2,1)} %get-tuple-element.77), channel_id=1, source_target_pairs={{80,0},{88,8},{64,16},{72,24},{112,32},{120,40},{96,48},{104,56},{... | collective-permute-start | bytes 1572872 | tf_op jit(solution)/shard_map/ppermute | solution.py:475
  159.9 38.7 %collective-permute-start.36 = (bf16[2,64,2048]{2,1,0:T(8,128)(2,1)}, bf16[2,64,2048]{2,1,0:T(8,128)(2,1)S(1)}, u32[]{:S(2)}, u32[]{:S(2)}) collective-permute-start(bf16[2,64,2048]{2,1,0:T(8,128)(2,1)} %get-tuple-element.78), channel_id=1, source_target_pairs={{48,0},{56,8},{32,16},{40,24},{80,32},{88,40},{64,48},{72,56},{112... | collective-permute-start | bytes 1572872 | tf_op jit(solution)/shard_map/ppermute | solution.py:475
  160.7 44.3 %collective-permute-start.37 = (bf16[2,64,2048]{2,1,0:T(8,128)(2,1)}, bf16[2,64,2048]{2,1,0:T(8,128)(2,1)S(1)}, u32[]{:S(2)}, u32[]{:S(2)}) collective-permute-start(bf16[2,64,2048]{2,1,0:T(8,128)(2,1)} %get-tuple-element.79), channel_id=1, source_target_pairs={{112,0},{120,8},{96,16},{104,24},{16,32},{24,40},{0,48},{8,56},{48... | collective-permute-start | bytes 1572872 | tf_op jit(solution)/shard_map/ppermute | solution.py:475
  190.8 35.5 %collective-permute-start.38 = (bf16[2,64,2048]{2,1,0:T(8,128)(2,1)}, bf16[2,64,2048]{2,1,0:T(8,128)(2,1)}, u32[]{:S(2)}, u32[]{:S(2)}) collective-permute-start(bf16[2,64,2048]{2,1,0:T(8,128)(2,1)} %get-tuple-element.80), channel_id=1, source_target_pairs={{72,0},{80,8},{88,16},{64,24},{104,32},{112,40},{120,48},{96,56},{... | collective-permute-start | bytes 1572872 | tf_op jit(solution)/shard_map/ppermute | solution.py:475
  198.6 37.8 %collective-permute-start.24 = (bf16[2,64,2048]{2,1,0:T(8,128)(2,1)}, bf16[2,64,2048]{2,1,0:T(8,128)(2,1)S(1)}, u32[]{:S(2)}, u32[]{:S(2)}) collective-permute-start(bf16[2,64,2048]{2,1,0:T(8,128)(2,1)} %get-tuple-element.63), channel_id=1, source_target_pairs={{40,0},{48,8},{56,16},{32,24},{72,32},{80,40},{88,48},{64,56},{104... | collective-permute-start | bytes 1572872 | tf_op jit(solution)/shard_map/ppermute | solution.py:475
  205.0 33.8 %collective-permute-start.25 = (bf16[2,64,2048]{2,1,0:T(8,128)(2,1)}, bf16[2,64,2048]{2,1,0:T(8,128)(2,1)S(1)}, u32[]{:S(2)}, u32[]{:S(2)}) collective-permute-start(bf16[2,64,2048]{2,1,0:T(8,128)(2,1)} %get-tuple-element.64), channel_id=1, source_target_pairs={{120,0},{96,8},{104,16},{112,24},{24,32},{0,40},{8,48},{16,56},{56... | collective-permute-start | bytes 1572872 | tf_op jit(solution)/shard_map/ppermute | solution.py:475
  227.7 31.6 %collective-permute-start.27 = (bf16[2,64,2048]{2,1,0:T(8,128)(2,1)S(1)}, bf16[2,64,2048]{2,1,0:T(8,128)(2,1)S(1)}, u32[]{:S(2)}, u32[]{:S(2)}) collective-permute-start(bf16[2,64,2048]{2,1,0:T(8,128)(2,1)S(1)} %copy-done.37), channel_id=1, source_target_pairs={{104,0},{112,8},{120,16},{96,24},{8,32},{16,40},{24,48},{0,56},{40... | collective-permute-start | bytes 1572872 | tf_op jit(solution)/shard_map/ppermute | solution.py:475
  236.5 43.0 %collective-permute-start.28 = (bf16[2,64,2048]{2,1,0:T(8,128)(2,1)S(1)}, bf16[2,64,2048]{2,1,0:T(8,128)(2,1)S(1)}, u32[]{:S(2)}, u32[]{:S(2)}) collective-permute-start(bf16[2,64,2048]{2,1,0:T(8,128)(2,1)S(1)} %copy-done.34), channel_id=1, source_target_pairs={{16,0},{24,8},{0,16},{8,24},{48,32},{56,40},{32,48},{40,56},{80,64... | collective-permute-start | bytes 1572872 | tf_op jit(solution)/shard_map/ppermute | solution.py:475
  238.9 40.6 %collective-permute-start.29 = (bf16[2,64,2048]{2,1,0:T(8,128)(2,1)S(1)}, bf16[2,64,2048]{2,1,0:T(8,128)(2,1)S(1)}, u32[]{:S(2)}, u32[]{:S(2)}) collective-permute-start(bf16[2,64,2048]{2,1,0:T(8,128)(2,1)S(1)} %copy-done.32), channel_id=1, source_target_pairs={{64,0},{72,8},{80,16},{88,24},{96,32},{104,40},{112,48},{120,56},{... | collective-permute-start | bytes 1572872 | tf_op jit(solution)/shard_map/ppermute | solution.py:475
  254.3 43.0 %collective-permute-start.14 = (bf16[2,64,2048]{2,1,0:T(8,128)(2,1)}, bf16[2,64,2048]{2,1,0:T(8,128)(2,1)S(1)}, u32[]{:S(2)}, u32[]{:S(2)}) collective-permute-start(bf16[2,64,2048]{2,1,0:T(8,128)(2,1)} %get-tuple-element.52), channel_id=1, source_target_pairs={{8,0},{16,8},{24,16},{0,24},{40,32},{48,40},{56,48},{32,56},{72,64... | collective-permute-start | bytes 1572872 | tf_op jit(solution)/shard_map/ppermute | solution.py:475
  259.4 37.9 %collective-permute-start.15 = (bf16[2,64,2048]{2,1,0:T(8,128)(2,1)}, bf16[2,64,2048]{2,1,0:T(8,128)(2,1)S(1)}, u32[]{:S(2)}, u32[]{:S(2)}) collective-permute-start(bf16[2,64,2048]{2,1,0:T(8,128)(2,1)} %get-tuple-element.53), channel_id=1, source_target_pairs={{24,0},{0,8},{8,16},{16,24},{56,32},{32,40},{40,48},{48,56},{88,64... | collective-permute-start | bytes 1572872 | tf_op jit(solution)/shard_map/ppermute | solution.py:475
  (57 other events, 1590.2 us)

commit v3 on v2

--- a/solution.py
+++ b/solution.py
@@ -21,7 +21,8 @@
 KEY_BLOCK = 2048
 ROW_TILE = 512
 SIDE = 4
-GROUPS = ((0, 10, 6, 14, 9, 11), (5, 15, 7, 13, 2, 8), (1, 3, 4, 12))
+GROUPS = ((0, 1, 3, 2, 4, 12, 8), (5, 15, 7, 13), (10, 6, 14, 9, 11))
+BACK = (GROUPS[0] + GROUPS[1], GROUPS[2])
 SAFE_LIMIT = 60.0
 VMEM = 56 * 1024 * 1024
 
@@ -228,7 +229,8 @@
     holder = routes // EXP_DEV
     down = (holder // SIDE - here_ref[0] + SIDE) % SIDE
     across = (holder % SIDE - here_ref[1] + SIDE) % SIDE
-    return (down * SIDE + across) * EXP_DEV + routes % EXP_DEV
+    shift = down * here_ref[2] + across * here_ref[3]
+    return shift * EXP_DEV + routes % EXP_DEV
 
 
 def route_body(here_ref, x_ref, gain_ref, routes_ref, *refs, group):
@@ -333,7 +335,7 @@
         named_ref[1:2, :] == expert, weights_ref[1:2, :], 0.0
     )
     slot = lax.broadcasted_iota(jnp.int32, (CAP, tokens), 0).astype(f32)
-    for group, out_ref in zip(GROUPS, out_refs):
+    for group, out_ref in zip(BACK, out_refs):
         for index, shift in enumerate(group):
             tiles = []
             for which in range(EXP_DEV):
@@ -352,7 +354,7 @@
     return pl.pallas_call(
         shares_body,
         out_shape=[
-            jax.ShapeDtypeStruct((2 * tokens, len(group) * LANES), bf16) for group in GROUPS
+            jax.ShapeDtypeStruct((2 * tokens, len(group) * LANES), bf16) for group in BACK
         ],
         compiler_params=params(),
         cost_estimate=cost(4e9, 4 * 2**20),
@@ -458,7 +460,8 @@
     owners, sides = lax.axis_size("ep"), lax.axis_size("tp") // 2
     ep = lax.axis_index("ep")
     offset = (ep * lax.axis_size("tp") + lax.axis_index("tp")) * own
-    here = jnp.stack([ep >> 2, ep & 3]).astype(jnp.int32)
+    core = lax.axis_index("tp") & 1
+    here = jnp.stack([ep >> 2, ep & 3, SIDE - 3 * core, 1 + 3 * core]).astype(jnp.int32)
     cosine, sine = tables(offset, own)
     gain = mixer_gain.reshape(1, D)
     bound = (
@@ -466,13 +469,16 @@
     ).reshape(1)
 
     def shifted(array, shift, back=False):
-        down, across = divmod(shift, SIDE)
         pairs = []
-        for z in range(SIDE):
-            for x in range(SIDE):
-                pair = (z * SIDE + x, (z + down) % SIDE * SIDE + (x + across) % SIDE)
-                pairs.append(pair[::-1] if back else pair)
-        return lax.ppermute(array, "ep", pairs)
+        for source in range(owners * 2 * sides):
+            holder, member = divmod(source, 2 * sides)
+            turns = divmod(shift, SIDE)
+            down, across = turns[::-1] if member & 1 else turns
+            z, x = divmod(holder, SIDE)
+            target = (z + down) % SIDE * SIDE + (x + across) % SIDE
+            pair = (source, target * 2 * sides + member)
+            pairs.append(pair[::-1] if back else pair)
+        return lax.ppermute(array, ("ep", "tp"), pairs)
 
     keyvals = pl.pallas_call(
         keyval_body,
@@ -526,9 +532,9 @@
     attended = attend(bound, queries, far, state, own, True)
     mixer_out = jnp.dot(attended, output_weight, preferred_element_type=f32).astype(bf16)
     total = None
-    for number, group in enumerate(GROUPS):
+    for number, group in enumerate(BACK):
         arrays = [returned[shift] for shift in group]
-        total = combine(share[number], arrays, total, number == len(GROUPS) - 1)
+        total = combine(share[number], arrays, total, number == len(BACK) - 1)
     return (mixer_out, total)
 
 

time: 603 us -> 590 us (0.978)
  the two profiles are of different devices: /device:TPU:64 before, /device:TPU:57 now
where the time goes in v3:
time: 590 us
  Pallas kernels  366 us (62%)
  starting transfers between devices  139 us (24%)
  waiting for transfers between devices  67.7 us (11%)
  local copies, waits for them, and re-layouts  9.62 us (2%)
    pallas_call x2, Pallas kernels, attend(): pl.pallas_call(functools.partial(attend_body, own=own, first=first, last=...  295 us
    ppermute x36, starting transfers between devices, shifted(): return lax.ppermute(array, ('ep', 'tp'), pairs)  132 us
    ppermute x36, waiting for transfers between devices, shifted(): return lax.ppermute(array, ('ep', 'tp'), pairs)  65.8 us
    pallas_call x3, Pallas kernels, expert(): pl.pallas_call(expert_body, grid=(EXP_DEV,), in_specs=[pl.BlockSpec((1, D...  27.3 us
    pallas_call x2, Pallas kernels, combine(): pl.pallas_call(functools.partial(combine_body, first=part is None), grid=...  18.5 us
  transfers between devices with their start and end apart: 40, of which 9 were waited for; matrix products, arithmetic and copies ran while one was open for 2% of the time, Pallas kernels for 37%

profile of v3, /device:TPU:57, one launch (start us, length us, event | category | flops | bytes accessed | tf_op | source)
XLA Modules:
  0.0 589.8 jit_solution(6343538271454830079)
XLA Ops:
  9.8 6.9 %route.1 = (bf16[2,64,2048]{2,1,0:T(8,128)(2,1)}, bf16[2,64,2048]{2,1,0:T(8,128)(2,1)}, bf16[2,64,2048]{2,1,0:T(8,128)(2,1)}, bf16[2,64,2048]{2,1,0:T(8,128)(2,1...) custom-call(s32[4]{0:T(128)} %pad_add_fusion.here_ref, ...), custom_call_target="tpu_custom_call" | custom-call | flops 8000000000 | bytes 8388608 | tf_op jit(solution)/shard_map/route/pallas_call | solution.py:273
  16.8 6.0 %dispatch.1 = (bf16[2,64,2048]{2,1,0:T(8,128)(2,1)}, bf16[2,64,2048]{2,1,0:T(8,128)(2,1)}, bf16[2,64,2048]{2,1,0:T(8,128)(2,1)}, bf16[2,64,2048]{2,1,0:T(8,128)(...) custom-call(f32[32,512]{1,0:T(8,128)} %get-tuple-element.43.place_re, ...), custom_call_target="tpu_custom_call" | custom-call | flops 5000000000 | bytes 6291456 | tf_op jit(solution)/shard_map/dispatch/pallas_call | solution.py:315
  33.8 10.4 %collective-permute-done.3 = bf16[512,256]{1,0:T(8,128)(2,1)S(1)} collective-permute-done((bf16[512,256]{1,0:T(8,128)(2,1)S(1)}, bf16[512,256]{1,0:T(8,128)(2,1)S(1)}, u32[]{:S(2)}, u32[]{:S(2)}) %collective-permute-start.3) | collective-permute-done | bytes 262176 | tf_op jit(solution)/shard_map/ppermute | solution.py:481
  46.4 14.5 %collective-permute-start.35 = (bf16[2,64,2048]{2,1,0:T(8,128)(2,1)}, bf16[2,64,2048]{2,1,0:T(8,128)(2,1)S(1)}, u32[]{:S(2)}, u32[]{:S(2)}) collective-permute-start(bf16[2,64,2048]{2,1,0:T(8,128)(2,1)} %get-tuple-element.75), channel_id=1, source_target_pairs={{0,104},{1,57},{2,106},{3,59},{4,108},{5,61},{6,110},{7,63},{8,112... | collective-permute-start | bytes 1572872 | tf_op jit(solution)/shard_map/ppermute | solution.py:481
  64.3 14.0 %collective-permute-done.35.refs_3_ = bf16[2,64,2048]{2,1,0:T(8,128)(2,1)S(1)} collective-permute-done((bf16[2,64,2048]{2,1,0:T(8,128)(2,1)}, bf16[2,64,2048]{2,1,0:T(8,128)(2,1)S(1)}, u32[]{:S(2)}, u32[]{:S(2)}) %collective-permute-start.35) | collective-permute-done | bytes 524320 | tf_op jit(solution)/shard_map/ppermute | solution.py:481
  78.6 6.9 %collective-permute-start.24 = (bf16[2,64,2048]{2,1,0:T(8,128)(2,1)S(1)}, bf16[2,64,2048]{2,1,0:T(8,128)(2,1)S(1)}, u32[]{:S(2)}, u32[]{:S(2)}) collective-permute-start(bf16[2,64,2048]{2,1,0:T(8,128)(2,1)S(1)} %copy-done.24), channel_id=1, source_target_pairs={{0,96},{1,25},{2,98},{3,27},{4,100},{5,29},{6,102},{7,31},{8,104},... | collective-permute-start | bytes 1572872 | tf_op jit(solution)/shard_map/ppermute | solution.py:481
  89.5 8.2 %collective-permute-done.22.refs_3_ = bf16[2,64,2048]{2,1,0:T(8,128)(2,1)S(1)} collective-permute-done((bf16[2,64,2048]{2,1,0:T(8,128)(2,1)S(1)}, bf16[2,64,2048]{2,1,0:T(8,128)(2,1)S(1)}, u32[]{:S(2)}, u32[]{:S(2)}) %collective-permute-start.22) | collective-permute-done | bytes 524320 | tf_op jit(solution)/shard_map/ppermute | solution.py:481
  102.2 11.9 %collective-permute-done.24.refs_5_ = bf16[2,64,2048]{2,1,0:T(8,128)(2,1)S(1)} collective-permute-done((bf16[2,64,2048]{2,1,0:T(8,128)(2,1)S(1)}, bf16[2,64,2048]{2,1,0:T(8,128)(2,1)S(1)}, u32[]{:S(2)}, u32[]{:S(2)}) %collective-permute-start.24) | collective-permute-done | bytes 524320 | tf_op jit(solution)/shard_map/ppermute | solution.py:481
  116.2 7.2 %collective-permute-start.9 = (bf16[8192,256]{1,0:T(8,128)(2,1)}, bf16[8192,256]{1,0:T(8,128)(2,1)}, u32[]{:S(2)}, u32[]{:S(2)}) collective-permute-start(bf16[8192,256]{1,0:T(8,128)(2,1)} %constant_dynamic-update-slice_fusion.7.kv_ref), channel_id=1, source_target_pairs={{0,1},{1,0},{2,3},{3,2},{4,5},{5,4},{6,7},{7,6},{8,9},{9,8},{10,11... | collective-permute-start | bytes 12582920 | tf_op jit(solution)/shard_map/ppermute | solution.py:499
  123.4 8.0 %expert.5 = (bf16[2,64,2048]{2,1,0:T(8,128)(2,1)}, bf16[2,64,2048]{2,1,0:T(8,128)(2,1)}, bf16[2,64,2048]{2,1,0:T(8,128)(2,1)}, bf16[2,64,2048]{2,1,0:T(8,128)(2,1)}) custom-call(bf16[2,2048,512]{2,1,0:T(8,128)(2,1)} %gate_ref.5, bf16[2,2048,512]{2,1,0:T(8,128)(2,1)} %up_ref.5, bf16[2,512,2048]{2,1,0:T(8,128)(2,1)} %down_ref.5, ...), custom_call_target="tpu_custom_call" | custom-call | flops 3221225472 | bytes 14680064 | tf_op jit(solution)/shard_map/expert/pallas_call | solution.py:380
  131.6 17.9 %collective-permute-start.36 = (bf16[2,64,2048]{2,1,0:T(8,128)(2,1)}, bf16[2,64,2048]{2,1,0:T(8,128)(2,1)S(1)}, u32[]{:S(2)}, u32[]{:S(2)}) collective-permute-start(bf16[2,64,2048]{2,1,0:T(8,128)(2,1)} %get-tuple-element.76), channel_id=1, source_target_pairs={{40,0},{41,1},{42,2},{43,3},{44,4},{45,5},{46,6},{47,7},{48,8},{49... | collective-permute-start | bytes 1572872 | tf_op jit(solution)/shard_map/ppermute | solution.py:481
  155.2 10.6 %expert.4 = (bf16[2,64,2048]{2,1,0:T(8,128)(2,1)}, bf16[2,64,2048]{2,1,0:T(8,128)(2,1)}, bf16[2,64,2048]{2,1,0:T(8,128)(2,1)}, bf16[2,64,2048]{2,1,0:T(8,128)(2,...) custom-call(bf16[2,2048,512]{2,1,0:T(8,128)(2,1)} %gate_ref.5, ...), custom_call_target="tpu_custom_call" | custom-call | flops 5637144576 | bytes 14680064 | tf_op jit(solution)/shard_map/expert/pallas_call | solution.py:380
  171.7 8.3 %collective-permute-start.27 = (bf16[2,64,2048]{2,1,0:T(8,128)(2,1)}, bf16[2,64,2048]{2,1,0:T(8,128)(2,1)}, u32[]{:S(2)}, u32[]{:S(2)}) collective-permute-start(bf16[2,64,2048]{2,1,0:T(8,128)(2,1)} %get-tuple-element.67), channel_id=1, source_target_pairs={{24,0},{97,1},{26,2},{99,3},{28,4},{101,5},{30,6},{103,7},{0,8},{1... | collective-permute-start | bytes 1572872 | tf_op jit(solution)/shard_map/ppermute | solution.py:481
  180.0 10.0 %collective-permute-start.28 = (bf16[2,64,2048]{2,1,0:T(8,128)(2,1)}, bf16[2,64,2048]{2,1,0:T(8,128)(2,1)}, u32[]{:S(2)}, u32[]{:S(2)}) collective-permute-start(bf16[2,64,2048]{2,1,0:T(8,128)(2,1)} %get-tuple-element.68), channel_id=1, source_target_pairs={{16,0},{65,1},{18,2},{67,3},{20,4},{69,5},{22,6},{71,7},{24,8},{73... | collective-permute-start | bytes 1572872 | tf_op jit(solution)/shard_map/ppermute | solution.py:481
  191.2 8.7 %expert.3 = (bf16[2,64,2048]{2,1,0:T(8,128)(2,1)}, bf16[2,64,2048]{2,1,0:T(8,128)(2,1)}, bf16[2,64,2048]{2,1,0:T(8,128)(2,1)}, bf16[2,64,2048]{2,1,0:T(8,128)(2,1)}, bf16[2,64,2048]{2,1,0:T(8,128)(2,1)}) custom-call(bf16[2,2048,512]{2,1,0:T(8,128)(2,1)} %gate_ref.5, bf16[2,2048,512]{2,1,0:T(8,128)(2,1)} %up_ref.5, bf16[2,512,2048]{2,1,0:T(8,128)(2,1)} %down_ref.5, ...), custom_call_target="tpu_custom_call" | custom-call | flops 4026531840 | bytes 14680064 | tf_op jit(solution)/shard_map/expert/pallas_call | solution.py:380
  201.6 9.7 %collective-permute-start.31 = (bf16[2,64,2048]{2,1,0:T(8,128)(2,1)}, bf16[2,64,2048]{2,1,0:T(8,128)(2,1)S(1)}, u32[]{:S(2)}, u32[]{:S(2)}) collective-permute-start(bf16[2,64,2048]{2,1,0:T(8,128)(2,1)} %get-tuple-element.71), channel_id=1, source_target_pairs={{64,0},{17,1},{66,2},{19,3},{68,4},{21,5},{70,6},{23,7},{72,8},{25... | collective-permute-start | bytes 1572872 | tf_op jit(solution)/shard_map/ppermute | solution.py:481
  214.3 5.7 query.1.q_ref
  226.5 22.6 %collective-permute-start.17 = (bf16[2,64,2048]{2,1,0:T(8,128)(2,1)S(1)}, bf16[2,64,2048]{2,1,0:T(8,128)(2,1)S(1)}, u32[]{:S(2)}, u32[]{:S(2)}) collective-permute-start(bf16[2,64,2048]{2,1,0:T(8,128)(2,1)S(1)} %copy-done.40), channel_id=1, source_target_pairs={{112,0},{89,1},{114,2},{91,3},{116,4},{93,5},{118,6},{95,7},{120,8... | collective-permute-start | bytes 1572872 | tf_op jit(solution)/shard_map/ppermute | solution.py:481
  253.1 10.9 %combine.2.refs_5_ = f32[512,2048]{1,0:T(8,128)} custom-call(bf16[1024,1408]{1,0:T(8,128)(2,1)} %get-tuple-element.57.share_ref, bf16[2,64,2048]{2,1,0:T(8,128)(2,1)} %get-tuple-element.65.refs_0_, bf16[2,64,2048]{2,1,0:T(8,128)(2,1)} %collective-permute-done.26.refs_1_, bf16[2,64,2048]{2,1,0:T(8,128)(2,1)} %collective-permute-done.27.refs_2_, ...), custom_call_target="tpu_custom_call" | custom-call | flops 5905580032 | bytes 8388608 | tf_op jit(solution)/shard_map/combine/pallas_call | solution.py:418
  264.3 11.4 %collective-permute-done.18.refs_3_ = bf16[2,64,2048]{2,1,0:T(8,128)(2,1)S(1)} collective-permute-done((bf16[2,64,2048]{2,1,0:T(8,128)(2,1)S(1)}, bf16[2,64,2048]{2,1,0:T(8,128)(2,1)S(1)}, u32[]{:S(2)}, u32[]{:S(2)}) %collective-permute-start.18) | collective-permute-done | bytes 524320 | tf_op jit(solution)/shard_map/ppermute | solution.py:481
  275.6 8.6 %collective-permute-done.19.refs_4_ = bf16[2,64,2048]{2,1,0:T(8,128)(2,1)S(1)} collective-permute-done((bf16[2,64,2048]{2,1,0:T(8,128)(2,1)S(1)}, bf16[2,64,2048]{2,1,0:T(8,128)(2,1)S(1)}, u32[]{:S(2)}, u32[]{:S(2)}) %collective-permute-start.19) | collective-permute-done | bytes 524320 | tf_op jit(solution)/shard_map/ppermute | solution.py:481
  285.0 7.6 %combine.3 = bf16[512,2048]{1,0:T(8,128)(2,1)} custom-call(bf16[1024,640]{1,0:T(8,128)(2,1)} %get-tuple-element.45.share_ref, bf16[2,64,2048]{2,1,0:T(8,128)(2,1)} %copy-done.6, bf16[2,64,2048]{2,1,0:T(8,128)(2,1)} %copy-done.7, bf16[2,64,2048]{2,1,0:T(8,128)(2,1)} %copy-done.8, bf16[2,64,2048]{2,1,0:T(8,128)(2,1)} %copy-done.9, ...), custom_call_target="tpu_custom_call" | custom-call | flops 2684354560 | bytes 8388608 | tf_op jit(solution)/shard_map/combine/pallas_call | solution.py:418
  292.7 147.1 %attend.2 = (f32[2048,128]{1,0:T(8,128)}, f32[2048,256]{1,0:T(8,128)}) custom-call(f32[1]{0:T(128)} %bitcast.safe_ref, bf16[2048,256]{1,0:T(8,128)(2,1)} %query.1.q_ref, bf16[8192,256]{1,0:T(8,128)(2,1)} %constant_dynamic-update-slice_fusion.7.kv_ref), custom_call_target="tpu_custom_call" | custom-call | flops 17179869184 | bytes 4194304 | tf_op jit(solution)/shard_map/attend/pallas_call | solution.py:192
  439.8 147.5 %attend.3 = bf16[128,1024]{1,0:T(8,128)(2,1)} custom-call(f32[1]{0:T(128)} %bitcast.safe_ref, bf16[2048,256]{1,0:T(8,128)(2,1)} %query.1.q_ref, bf16[8192,256]{1,0:T(8,128)(2,1)} %collective-permute-done.9.kv_ref, f32[2048,128]{1,0:T(8,128)} %get-tuple-element.41.refs_0_, f32[2048,256]{1,0:T(8,128)} %get-tuple-element.42.refs_1_), custom_call_target="tpu_custom_call" | custom-call | flops 17179869184 | bytes 4194304 | tf_op jit(solution)/shard_map/attend/pallas_call | solution.py:192
  (182 shorter events, 66.8 us)
Async XLA Ops:
  22.8 38.1 %collective-permute-start.32 = (bf16[2,64,2048]{2,1,0:T(8,128)(2,1)}, bf16[2,64,2048]{2,1,0:T(8,128)(2,1)S(1)}, u32[]{:S(2)}, u32[]{:S(2)}) collective-permute-start(bf16[2,64,2048]{2,1,0:T(8,128)(2,1)} %get-tuple-element.72), channel_id=1, source_target_pairs={{0,40},{1,41},{2,42},{3,43},{4,44},{5,45},{6,46},{7,47},{8,48},{9,... | collective-permute-start | bytes 1572872 | tf_op jit(solution)/shard_map/ppermute | solution.py:481
  24.5 36.4 %collective-permute-start.33 = (bf16[2,64,2048]{2,1,0:T(8,128)(2,1)}, bf16[2,64,2048]{2,1,0:T(8,128)(2,1)S(1)}, u32[]{:S(2)}, u32[]{:S(2)}) collective-permute-start(bf16[2,64,2048]{2,1,0:T(8,128)(2,1)} %get-tuple-element.73), channel_id=1, source_target_pairs={{0,120},{1,121},{2,122},{3,123},{4,124},{5,125},{6,126},{7,127},{8... | collective-permute-start | bytes 1572872 | tf_op jit(solution)/shard_map/ppermute | solution.py:481
  46.4 32.2 %collective-permute-start.6 = (bf16[2048,256]{1,0:T(8,128)(2,1)S(1)}, bf16[2048,256]{1,0:T(8,128)(2,1)S(1)}, u32[]{:S(2)}, u32[]{:S(2)}) collective-permute-start(bf16[2048,256]{1,0:T(8,128)(2,1)S(1)} %get-tuple-element.80), channel_id=1, source_target_pairs={{0,2},{1,3},{2,4},{3,5},{4,6},{5,7},{6,0},{7,1},{8,10},{9,11},{10,... | collective-permute-start | bytes 3145736 | tf_op jit(solution)/shard_map/ppermute | solution.py:497
  46.4 31.9 %collective-permute-start.35 = (bf16[2,64,2048]{2,1,0:T(8,128)(2,1)}, bf16[2,64,2048]{2,1,0:T(8,128)(2,1)S(1)}, u32[]{:S(2)}, u32[]{:S(2)}) collective-permute-start(bf16[2,64,2048]{2,1,0:T(8,128)(2,1)} %get-tuple-element.75), channel_id=1, source_target_pairs={{0,104},{1,57},{2,106},{3,59},{4,108},{5,61},{6,110},{7,63},{8,112... | collective-permute-start | bytes 1572872 | tf_op jit(solution)/shard_map/ppermute | solution.py:481
  78.2 35.8 %collective-permute-start.8 = (bf16[2048,256]{1,0:T(8,128)(2,1)S(1)}, bf16[2048,256]{1,0:T(8,128)(2,1)S(1)}, u32[]{:S(2)}, u32[]{:S(2)}) collective-permute-start(bf16[2048,256]{1,0:T(8,128)(2,1)S(1)} %get-tuple-element.80), channel_id=1, source_target_pairs={{0,6},{1,7},{2,0},{3,1},{4,2},{5,3},{6,4},{7,5},{8,14},{9,15},{10,... | collective-permute-start | bytes 3145736 | tf_op jit(solution)/shard_map/ppermute | solution.py:497
  78.6 35.5 %collective-permute-start.24 = (bf16[2,64,2048]{2,1,0:T(8,128)(2,1)S(1)}, bf16[2,64,2048]{2,1,0:T(8,128)(2,1)S(1)}, u32[]{:S(2)}, u32[]{:S(2)}) collective-permute-start(bf16[2,64,2048]{2,1,0:T(8,128)(2,1)S(1)} %copy-done.24), channel_id=1, source_target_pairs={{0,96},{1,25},{2,98},{3,27},{4,100},{5,29},{6,102},{7,31},{8,104},... | collective-permute-start | bytes 1572872 | tf_op jit(solution)/shard_map/ppermute | solution.py:481
  87.3 28.1 %collective-permute-start.25 = (bf16[2,64,2048]{2,1,0:T(8,128)(2,1)S(1)}, bf16[2,64,2048]{2,1,0:T(8,128)(2,1)S(1)}, u32[]{:S(2)}, u32[]{:S(2)}) collective-permute-start(bf16[2,64,2048]{2,1,0:T(8,128)(2,1)S(1)} %copy-done.23), channel_id=1, source_target_pairs={{0,64},{1,17},{2,66},{3,19},{4,68},{5,21},{6,70},{7,23},{8,72},{9,... | collective-permute-start | bytes 1572872 | tf_op jit(solution)/shard_map/ppermute | solution.py:481
  97.6 33.8 %collective-permute-start.10 = (bf16[2,64,2048]{2,1,0:T(8,128)(2,1)S(1)}, bf16[2,64,2048]{2,1,0:T(8,128)(2,1)S(1)}, u32[]{:S(2)}, u32[]{:S(2)}) collective-permute-start(bf16[2,64,2048]{2,1,0:T(8,128)(2,1)S(1)} %copy-done.22), channel_id=1, source_target_pairs={{0,80},{1,81},{2,82},{3,83},{4,84},{5,85},{6,86},{7,87},{8,88},{9,... | collective-permute-start | bytes 1572872 | tf_op jit(solution)/shard_map/ppermute | solution.py:481
  97.7 34.0 %collective-permute-start.11 = (bf16[2,64,2048]{2,1,0:T(8,128)(2,1)S(1)}, bf16[2,64,2048]{2,1,0:T(8,128)(2,1)S(1)}, u32[]{:S(2)}, u32[]{:S(2)}) collective-permute-start(bf16[2,64,2048]{2,1,0:T(8,128)(2,1)S(1)} %copy-done.21), channel_id=1, source_target_pairs={{0,48},{1,73},{2,50},{3,75},{4,52},{5,77},{6,54},{7,79},{8,56},{9,... | collective-permute-start | bytes 1572872 | tf_op jit(solution)/shard_map/ppermute | solution.py:481
  114.0 35.5 %collective-permute-start.12 = (bf16[2,64,2048]{2,1,0:T(8,128)(2,1)S(1)}, bf16[2,64,2048]{2,1,0:T(8,128)(2,1)S(1)}, u32[]{:S(2)}, u32[]{:S(2)}) collective-permute-start(bf16[2,64,2048]{2,1,0:T(8,128)(2,1)S(1)} %copy-done.20), channel_id=1, source_target_pairs={{0,112},{1,89},{2,114},{3,91},{4,116},{5,93},{6,118},{7,95},{8,120... | collective-permute-start | bytes 1572872 | tf_op jit(solution)/shard_map/ppermute | solution.py:481
  114.1 35.5 %collective-permute-start.13 = (bf16[2,64,2048]{2,1,0:T(8,128)(2,1)S(1)}, bf16[2,64,2048]{2,1,0:T(8,128)(2,1)S(1)}, u32[]{:S(2)}, u32[]{:S(2)}) collective-permute-start(bf16[2,64,2048]{2,1,0:T(8,128)(2,1)S(1)} %copy-done.19), channel_id=1, source_target_pairs={{0,72},{1,49},{2,74},{3,51},{4,76},{5,53},{6,78},{7,55},{8,80},{9,... | collective-permute-start | bytes 1572872 | tf_op jit(solution)/shard_map/ppermute | solution.py:481
  116.2 323.6 %collective-permute-start.9 = (bf16[8192,256]{1,0:T(8,128)(2,1)}, bf16[8192,256]{1,0:T(8,128)(2,1)}, u32[]{:S(2)}, u32[]{:S(2)}) collective-permute-start(bf16[8192,256]{1,0:T(8,128)(2,1)} %constant_dynamic-update-slice_fusion.7.kv_ref), channel_id=1, source_target_pairs={{0,1},{1,0},{2,3},{3,2},{4,5},{5,4},{6,7},{7,6},{8,9},{9,8},{10,11... | collective-permute-start | bytes 12582920 | tf_op jit(solution)/shard_map/ppermute | solution.py:499
  131.4 34.4 %collective-permute-start.14 = (bf16[2,64,2048]{2,1,0:T(8,128)(2,1)S(1)}, bf16[2,64,2048]{2,1,0:T(8,128)(2,1)S(1)}, u32[]{:S(2)}, u32[]{:S(2)}) collective-permute-start(bf16[2,64,2048]{2,1,0:T(8,128)(2,1)S(1)} %copy-done.18), channel_id=1, source_target_pairs={{0,88},{1,113},{2,90},{3,115},{4,92},{5,117},{6,94},{7,119},{8,64}... | collective-permute-start | bytes 1572872 | tf_op jit(solution)/shard_map/ppermute | solution.py:481
  131.6 35.5 %collective-permute-start.36 = (bf16[2,64,2048]{2,1,0:T(8,128)(2,1)}, bf16[2,64,2048]{2,1,0:T(8,128)(2,1)S(1)}, u32[]{:S(2)}, u32[]{:S(2)}) collective-permute-start(bf16[2,64,2048]{2,1,0:T(8,128)(2,1)} %get-tuple-element.76), channel_id=1, source_target_pairs={{40,0},{41,1},{42,2},{43,3},{44,4},{45,5},{46,6},{47,7},{48,8},{49... | collective-permute-start | bytes 1572872 | tf_op jit(solution)/shard_map/ppermute | solution.py:481
  149.5 30.5 %collective-permute-start.38 = (bf16[2,64,2048]{2,1,0:T(8,128)(2,1)}, bf16[2,64,2048]{2,1,0:T(8,128)(2,1)S(1)}, u32[]{:S(2)}, u32[]{:S(2)}) collective-permute-start(bf16[2,64,2048]{2,1,0:T(8,128)(2,1)} %get-tuple-element.78), channel_id=1, source_target_pairs={{56,0},{105,1},{58,2},{107,3},{60,4},{109,5},{62,6},{111,7},{32,8}... | collective-permute-start | bytes 1572872 | tf_op jit(solution)/shard_map/ppermute | solution.py:481
  165.8 34.2 %collective-permute-start.39 = (bf16[2,64,2048]{2,1,0:T(8,128)(2,1)}, bf16[2,64,2048]{2,1,0:T(8,128)(2,1)S(1)}, u32[]{:S(2)}, u32[]{:S(2)}) collective-permute-start(bf16[2,64,2048]{2,1,0:T(8,128)(2,1)} %get-tuple-element.79), channel_id=1, source_target_pairs={{104,0},{57,1},{106,2},{59,3},{108,4},{61,5},{110,6},{63,7},{112,8... | collective-permute-start | bytes 1572872 | tf_op jit(solution)/shard_map/ppermute | solution.py:481
  167.1 33.0 %collective-permute-start.26 = (bf16[2,64,2048]{2,1,0:T(8,128)(2,1)}, bf16[2,64,2048]{2,1,0:T(8,128)(2,1)}, u32[]{:S(2)}, u32[]{:S(2)}) collective-permute-start(bf16[2,64,2048]{2,1,0:T(8,128)(2,1)} %get-tuple-element.66), channel_id=1, source_target_pairs={{8,0},{33,1},{10,2},{35,3},{12,4},{37,5},{14,6},{39,7},{16,8},{41,... | collective-permute-start | bytes 1572872 | tf_op jit(solution)/shard_map/ppermute | solution.py:481
  171.7 29.8 %collective-permute-start.27 = (bf16[2,64,2048]{2,1,0:T(8,128)(2,1)}, bf16[2,64,2048]{2,1,0:T(8,128)(2,1)}, u32[]{:S(2)}, u32[]{:S(2)}) collective-permute-start(bf16[2,64,2048]{2,1,0:T(8,128)(2,1)} %get-tuple-element.67), channel_id=1, source_target_pairs={{24,0},{97,1},{26,2},{99,3},{28,4},{101,5},{30,6},{103,7},{0,8},{1... | collective-permute-start | bytes 1572872 | tf_op jit(solution)/shard_map/ppermute | solution.py:481
  180.0 31.3 %collective-permute-start.28 = (bf16[2,64,2048]{2,1,0:T(8,128)(2,1)}, bf16[2,64,2048]{2,1,0:T(8,128)(2,1)}, u32[]{:S(2)}, u32[]{:S(2)}) collective-permute-start(bf16[2,64,2048]{2,1,0:T(8,128)(2,1)} %get-tuple-element.68), channel_id=1, source_target_pairs={{16,0},{65,1},{18,2},{67,3},{20,4},{69,5},{22,6},{71,7},{24,8},{73... | collective-permute-start | bytes 1572872 | tf_op jit(solution)/shard_map/ppermute | solution.py:481
  201.6 47.5 %collective-permute-start.31 = (bf16[2,64,2048]{2,1,0:T(8,128)(2,1)}, bf16[2,64,2048]{2,1,0:T(8,128)(2,1)S(1)}, u32[]{:S(2)}, u32[]{:S(2)}) collective-permute-start(bf16[2,64,2048]{2,1,0:T(8,128)(2,1)} %get-tuple-element.71), channel_id=1, source_target_pairs={{64,0},{17,1},{66,2},{19,3},{68,4},{21,5},{70,6},{23,7},{72,8},{25... | collective-permute-start | bytes 1572872 | tf_op jit(solution)/shard_map/ppermute | solution.py:481
  211.3 38.2 %collective-permute-start.15 = (bf16[2,64,2048]{2,1,0:T(8,128)(2,1)}, bf16[2,64,2048]{2,1,0:T(8,128)(2,1)S(1)}, u32[]{:S(2)}, u32[]{:S(2)}) collective-permute-start(bf16[2,64,2048]{2,1,0:T(8,128)(2,1)} %get-tuple-element.52), channel_id=1, source_target_pairs={{80,0},{81,1},{82,2},{83,3},{84,4},{85,5},{86,6},{87,7},{88,8},{89... | collective-permute-start | bytes 1572872 | tf_op jit(solution)/shard_map/ppermute | solution.py:481
  223.8 40.2 %collective-permute-start.16 = (bf16[2,64,2048]{2,1,0:T(8,128)(2,1)S(1)}, bf16[2,64,2048]{2,1,0:T(8,128)(2,1)S(1)}, u32[]{:S(2)}, u32[]{:S(2)}) collective-permute-start(bf16[2,64,2048]{2,1,0:T(8,128)(2,1)S(1)} %copy-done.41), channel_id=1, source_target_pairs={{48,0},{73,1},{50,2},{75,3},{52,4},{77,5},{54,6},{79,7},{56,8},{81... | collective-permute-start | bytes 1572872 | tf_op jit(solution)/shard_map/ppermute | solution.py:481
  226.5 37.8 %collective-permute-start.17 = (bf16[2,64,2048]{2,1,0:T(8,128)(2,1)S(1)}, bf16[2,64,2048]{2,1,0:T(8,128)(2,1)S(1)}, u32[]{:S(2)}, u32[]{:S(2)}) collective-permute-start(bf16[2,64,2048]{2,1,0:T(8,128)(2,1)S(1)} %copy-done.40), channel_id=1, source_target_pairs={{112,0},{89,1},{114,2},{91,3},{116,4},{93,5},{118,6},{95,7},{120,8... | collective-permute-start | bytes 1572872 | tf_op jit(solution)/shard_map/ppermute | solution.py:481
  249.5 34.7 %collective-permute-start.19 = (bf16[2,64,2048]{2,1,0:T(8,128)(2,1)S(1)}, bf16[2,64,2048]{2,1,0:T(8,128)(2,1)S(1)}, u32[]{:S(2)}, u32[]{:S(2)}) collective-permute-start(bf16[2,64,2048]{2,1,0:T(8,128)(2,1)S(1)} %copy-done.37), channel_id=1, source_target_pairs={{88,0},{113,1},{90,2},{115,3},{92,4},{117,5},{94,6},{119,7},{64,8}... | collective-permute-start | bytes 1572872 | tf_op jit(solution)/shard_map/ppermute | solution.py:481
  (61 other events, 1918.0 us)

commit v4 on v3

--- a/solution.py
+++ b/solution.py
@@ -21,7 +21,7 @@
 KEY_BLOCK = 2048
 ROW_TILE = 512
 SIDE = 4
-GROUPS = ((0, 1, 3, 2, 4, 12, 8), (5, 15, 7, 13), (10, 6, 14, 9, 11))
+GROUPS = ((0, 1, 3, 4, 12), (2, 8, 5, 15, 7, 13), (10, 6, 14, 9, 11))
 BACK = (GROUPS[0] + GROUPS[1], GROUPS[2])
 SAFE_LIMIT = 60.0
 VMEM = 56 * 1024 * 1024
@@ -73,8 +73,10 @@
     normed = normed_rows(x_ref[...], gain_ref[...])
     keys = jnp.dot(normed, kw_ref[...], preferred_element_type=f32)
     values = jnp.dot(normed, vw_ref[...], preferred_element_type=f32)
-    out_ref[:, :LANES] = head_pair(keys, twice(kgain_ref[...]), cos_ref[...], sin_ref[...]).astype(bf16)
-    out_ref[:, LANES:] = values.astype(bf16)
+    keys = head_pair(keys, twice(kgain_ref[...]), cos_ref[...], sin_ref[...]).astype(bf16)
+    both = jnp.concatenate([keys, values.astype(bf16)], axis=1)
+    for index in range(out_ref.shape[0]):
+        out_ref[index] = both
 
 
 def query_body(x_ref, gain_ref, qw_ref, qgain_ref, cos_ref, sin_ref, out_ref):
@@ -341,12 +343,8 @@
             for which in range(EXP_DEV):
                 row = slice(shift * EXP_DEV + which, shift * EXP_DEV + which + 1)
                 tiles.append(jnp.where(place_ref[row, :] == slot, share[row, :], 0.0))
-            value = jnp.concatenate(tiles, axis=0).T
-            high = value.astype(bf16)
-            low = (value - high.astype(f32)).astype(bf16)
             columns = slice(index * LANES, (index + 1) * LANES)
-            out_ref[:tokens, columns] = high
-            out_ref[tokens:, columns] = low
+            out_ref[:, columns] = jnp.concatenate(tiles, axis=0).T.astype(bf16)
 
 
 def shares(place, named, weights):
@@ -354,7 +352,7 @@
     return pl.pallas_call(
         shares_body,
         out_shape=[
-            jax.ShapeDtypeStruct((2 * tokens, len(group) * LANES), bf16) for group in BACK
+            jax.ShapeDtypeStruct((tokens, len(group) * LANES), bf16) for group in BACK
         ],
         compiler_params=params(),
         cost_estimate=cost(4e9, 4 * 2**20),
@@ -397,17 +395,15 @@
 def combine_body(share_ref, *refs, first):
     out_ref = refs[-1]
     back_refs = refs[:-1] if first else refs[:-2]
-    tokens = out_ref.shape[0]
     back = jnp.concatenate([ref[...].reshape(-1, ref.shape[-1]) for ref in back_refs], axis=0)
-    both = jnp.dot(share_ref[...], back, preferred_element_type=f32)
-    total = both[:tokens] + both[tokens:]
+    total = jnp.dot(share_ref[...], back, preferred_element_type=f32)
     if not first:
         total = total + refs[-2][...]
     out_ref[...] = total.astype(out_ref.dtype)
 
 
 def combine(share, arrays, part, last):
-    tokens = share.shape[0] // 2
+    tokens = share.shape[0]
     block = 512
     column = pl.BlockSpec((tokens, block), lambda i: (0, i))
     specs = [pl.BlockSpec(share.shape, lambda i: (0, 0))] + bundles(len(arrays), block)[0]
@@ -482,15 +478,13 @@
 
     keyvals = pl.pallas_call(
         keyval_body,
-        out_shape=jax.ShapeDtypeStruct((own, 2 * LANES), bf16),
+        out_shape=jax.ShapeDtypeStruct((owners, own, 2 * LANES), bf16),
         compiler_params=params(),
         cost_estimate=cost(own * D * 512, 2 * 2**20),
         name="keyval",
     )(mixer_in, gain, key_weight, value_weight, key_gain.reshape(1, HEAD), cosine, sine)
-    line = jnp.concatenate(
-        [keyvals] + [shifted(keyvals, SIDE * turn) for turn in range(1, SIDE)], axis=0
-    )
-    plane = jnp.concatenate([line] + [shifted(line, turn) for turn in range(1, SIDE)], axis=0)
+    plane = lax.all_to_all(keyvals, "ep", split_axis=0, concat_axis=0, tiled=True)
+    plane = plane.reshape(owners * own, 2 * LANES)
     near = [plane]
     for turn in range(1, sides):
         ring = [(2 * y + c, 2 * ((y + turn) % sides) + c) for y in range(sides) for c in range(2)]

time: 590 us -> 568 us (0.963)
  the two profiles are of different devices: /device:TPU:57 before, /device:TPU:16 now
where the time goes in v4:
time: 568 us; the launch traced here: 564 us
  Pallas kernels  361 us (64%)
  waiting for transfers between devices  102 us (18%)
  starting transfers between devices  90.4 us (16%)
    pallas_call x2, Pallas kernels, attend(): pl.pallas_call(functools.partial(attend_body, own=own, first=first, last=...  295 us
    ppermute x30, waiting for transfers between devices, shifted(): return lax.ppermute(array, ('ep', 'tp'), pairs)  83.4 us
    ppermute x30, starting transfers between devices, shifted(): return lax.ppermute(array, ('ep', 'tp'), pairs)  79.8 us
    pallas_call x3, Pallas kernels, expert(): pl.pallas_call(expert_body, grid=(EXP_DEV,), in_specs=[pl.BlockSpec((1, D...  27.4 us
    ppermute x3, waiting for transfers between devices, per_device(): near.append(lax.ppermute(plane, 'tp', ring))  18.2 us
    pallas_call x2, Pallas kernels, combine(): pl.pallas_call(functools.partial(combine_body, first=part is None), grid=...  14.3 us
  transfers between devices with their start and end apart: 35, of which 12 were waited for; matrix products, arithmetic and copies ran while one was open for 1% of the time, Pallas kernels for 37%

profile of v4, /device:TPU:16, one launch (start us, length us, event | category | flops | bytes accessed | tf_op | source)
XLA Modules:
  0.0 563.7 jit_solution(13444070978850930354)
XLA Ops:
  4.9 7.9 %all-to-all-start = ((bf16[16,128,256]{2,1,0:T(8,128)(2,1)}), bf16[16,128,256]{2,1,0:T(8,128)(2,1)S(1)}, u32[]{:S(2)}, u32[]{:S(2)}) async-start(bf16[16,128,256]{2,1,0:T(8,128)(2,1)} %keyval.1), calls=%async_computation | async-start | bytes 2097152 | tf_op jit(solution)/shard_map/all_to_all | solution.py:486
  13.3 6.4 %route.1 = (bf16[2,64,2048]{2,1,0:T(8,128)(2,1)}, bf16[2,64,2048]{2,1,0:T(8,128)(2,1)}, bf16[2,64,2048]{2,1,0:T(8,128)(2,1)}, bf16[2,64,2048]{2,1,0:T(8,128)(2,1...) custom-call(s32[4]{0:T(128)} %pad_add_fusion.here_ref, ...), custom_call_target="tpu_custom_call" | custom-call | flops 8000000000 | bytes 8388608 | tf_op jit(solution)/shard_map/route/pallas_call | solution.py:275
  19.7 6.4 %dispatch.1 = (bf16[2,64,2048]{2,1,0:T(8,128)(2,1)}, bf16[2,64,2048]{2,1,0:T(8,128)(2,1)}, bf16[2,64,2048]{2,1,0:T(8,128)(2,1)}, bf16[2,64,2048]{2,1,0:T(8,128)(...) custom-call(f32[32,512]{1,0:T(8,128)} %get-tuple-element.43.place_re, ...), custom_call_target="tpu_custom_call" | custom-call | flops 5000000000 | bytes 6291456 | tf_op jit(solution)/shard_map/dispatch/pallas_call | solution.py:317
  41.4 5.4 collective-permute-start.27
  48.3 8.1 %collective-permute-done.24.refs_2_ = bf16[2,64,2048]{2,1,0:T(8,128)(2,1)S(1)} collective-permute-done((bf16[2,64,2048]{2,1,0:T(8,128)(2,1)}, bf16[2,64,2048]{2,1,0:T(8,128)(2,1)S(1)}, u32[]{:S(2)}, u32[]{:S(2)}) %collective-permute-start.24) | collective-permute-done | bytes 524320 | tf_op jit(solution)/shard_map/ppermute | solution.py:477
  58.3 9.1 %collective-permute-done.26.refs_4_ = bf16[2,64,2048]{2,1,0:T(8,128)(2,1)} collective-permute-done((bf16[2,64,2048]{2,1,0:T(8,128)(2,1)}, bf16[2,64,2048]{2,1,0:T(8,128)(2,1)}, u32[]{:S(2)}, u32[]{:S(2)}) %collective-permute-start.26) | collective-permute-done | bytes 524320 | tf_op jit(solution)/shard_map/ppermute | solution.py:477
  72.8 4.9 collective-permute-done.15.refs_2_
  85.4 18.2 %collective-permute-done = bf16[2048,256]{1,0:T(8,128)(2,1)S(1)} collective-permute-done((bf16[2048,256]{1,0:T(8,128)(2,1)S(1)}, bf16[2048,256]{1,0:T(8,128)(2,1)S(1)}, u32[]{:S(2)}, u32[]{:S(2)}) %collective-permute-start) | collective-permute-done | bytes 1048608 | tf_op jit(solution)/shard_map/ppermute | solution.py:491
  111.8 9.7 %expert.5 = (bf16[2,64,2048]{2,1,0:T(8,128)(2,1)}, bf16[2,64,2048]{2,1,0:T(8,128)(2,1)}, bf16[2,64,2048]{2,1,0:T(8,128)(2,1)}, bf16[2,64,2048]{2,1,0:T(8,128)(2,...) custom-call(bf16[2,2048,512]{2,1,0:T(8,128)(2,1)} %gate_ref.5, bf16[2,2048,512]{2,1,0:T(8,128)(2,1)} %up_ref.5, ...), custom_call_target="tpu_custom_call" | custom-call | flops 4831838208 | bytes 14680064 | tf_op jit(solution)/shard_map/expert/pallas_call | solution.py:378
  121.5 5.7 %collective-permute-start.8 = (bf16[2,64,2048]{2,1,0:T(8,128)(2,1)S(1)}, bf16[2,64,2048]{2,1,0:T(8,128)(2,1)S(1)}, u32[]{:S(2)}, u32[]{:S(2)}) collective-permute-start(bf16[2,64,2048]{2,1,0:T(8,128)(2,1)S(1)} %copy-done.12), channel_id=1, source_target_pairs={{0,88},{1,113},{2,90},{3,115},{4,92},{5,117},{6,94},{7,119},{8,64}... | collective-permute-start | bytes 1572872 | tf_op jit(solution)/shard_map/ppermute | solution.py:477
  130.7 17.8 %collective-permute-done.6.refs_2_ = bf16[2,64,2048]{2,1,0:T(8,128)(2,1)S(1)} collective-permute-done((bf16[2,64,2048]{2,1,0:T(8,128)(2,1)}, bf16[2,64,2048]{2,1,0:T(8,128)(2,1)S(1)}, u32[]{:S(2)}, u32[]{:S(2)}) %collective-permute-start.6) | collective-permute-done | bytes 524320 | tf_op jit(solution)/shard_map/ppermute | solution.py:477
  148.5 11.3 %collective-permute-done.7.refs_3_ = bf16[2,64,2048]{2,1,0:T(8,128)(2,1)S(1)} collective-permute-done((bf16[2,64,2048]{2,1,0:T(8,128)(2,1)}, bf16[2,64,2048]{2,1,0:T(8,128)(2,1)S(1)}, u32[]{:S(2)}, u32[]{:S(2)}) %collective-permute-start.7) | collective-permute-done | bytes 524320 | tf_op jit(solution)/shard_map/ppermute | solution.py:477
  159.8 8.9 %expert.4 = (bf16[2,64,2048]{2,1,0:T(8,128)(2,1)}, bf16[2,64,2048]{2,1,0:T(8,128)(2,1)}, bf16[2,64,2048]{2,1,0:T(8,128)(2,1)}, bf16[2,64,2048]{2,1,0:T(8,128)(2,1)}, bf16[2,64,2048]{2,1,0:T(8,128)(2,1)}) custom-call(bf16[2,2048,512]{2,1,0:T(8,128)(2,1)} %gate_ref.5, bf16[2,2048,512]{2,1,0:T(8,128)(2,1)} %up_ref.5, bf16[2,512,2048]{2,1,0:T(8,128)(2,1)} %down_ref.5, ...), custom_call_target="tpu_custom_call" | custom-call | flops 4026531840 | bytes 14680064 | tf_op jit(solution)/shard_map/expert/pallas_call | solution.py:378
  171.6 6.3 %collective-permute-start.33 = (bf16[2,64,2048]{2,1,0:T(8,128)(2,1)}, bf16[2,64,2048]{2,1,0:T(8,128)(2,1)}, u32[]{:S(2)}, u32[]{:S(2)}) collective-permute-start(bf16[2,64,2048]{2,1,0:T(8,128)(2,1)} %get-tuple-element.79), channel_id=1, source_target_pairs={{104,0},{57,1},{106,2},{59,3},{108,4},{61,5},{110,6},{63,7},{112,8... | collective-permute-start | bytes 1572872 | tf_op jit(solution)/shard_map/ppermute | solution.py:477
  179.2 8.7 %expert.3 = (bf16[2,64,2048]{2,1,0:T(8,128)(2,1)}, bf16[2,64,2048]{2,1,0:T(8,128)(2,1)}, bf16[2,64,2048]{2,1,0:T(8,128)(2,1)}, bf16[2,64,2048]{2,1,0:T(8,128)(2,1)}, bf16[2,64,2048]{2,1,0:T(8,128)(2,1)}) custom-call(bf16[2,2048,512]{2,1,0:T(8,128)(2,1)} %gate_ref.5, bf16[2,2048,512]{2,1,0:T(8,128)(2,1)} %up_ref.5, bf16[2,512,2048]{2,1,0:T(8,128)(2,1)} %down_ref.5, ...), custom_call_target="tpu_custom_call" | custom-call | flops 4026531840 | bytes 14680064 | tf_op jit(solution)/shard_map/expert/pallas_call | solution.py:378
  193.7 6.1 %collective-permute-start.10 = (bf16[2,64,2048]{2,1,0:T(8,128)(2,1)}, bf16[2,64,2048]{2,1,0:T(8,128)(2,1)S(1)}, u32[]{:S(2)}, u32[]{:S(2)}) collective-permute-start(bf16[2,64,2048]{2,1,0:T(8,128)(2,1)} %get-tuple-element.53), channel_id=1, source_target_pairs={{48,0},{73,1},{50,2},{75,3},{52,4},{77,5},{54,6},{79,7},{56,8},{81... | collective-permute-start | bytes 1572872 | tf_op jit(solution)/shard_map/ppermute | solution.py:477
  201.1 5.7 %query.1.q_ref = bf16[2048,256]{1,0:T(8,128)(2,1)} custom-call(bf16[128,2048]{1,0:T(8,128)(2,1)} %x_ref.4, f32[1,2048]{1,0:T(1,128)} %bitcast.19, bf16[2048,1024]{1,0:T(8,128)(2,1)} %qw_ref.1, f32[1,64]{1,0:T(1,128)} %bitcast.21, f32[128,128]{1,0:T(8,128)} %get-tuple-element.81.cos_ref, f32[128,128]{1,0:T(8,128)} %get-tuple-element.80.sin_ref), custom_call_target="tpu_custom_call" | custom-call | flops 536870912 | bytes 5242880 | tf_op jit(solution)/shard_map/query/pallas_call | solution.py:506
  210.1 9.0 %collective-permute-start.12 = (bf16[2,64,2048]{2,1,0:T(8,128)(2,1)S(1)}, bf16[2,64,2048]{2,1,0:T(8,128)(2,1)S(1)}, u32[]{:S(2)}, u32[]{:S(2)}) collective-permute-start(bf16[2,64,2048]{2,1,0:T(8,128)(2,1)S(1)} %copy-done.23), channel_id=1, source_target_pairs={{72,0},{49,1},{74,2},{51,3},{76,4},{53,5},{78,6},{55,7},{80,8},{57... | collective-permute-start | bytes 1572872 | tf_op jit(solution)/shard_map/ppermute | solution.py:477
  219.1 9.2 %collective-permute-start.9 = (bf16[2,64,2048]{2,1,0:T(8,128)(2,1)S(1)}, bf16[2,64,2048]{2,1,0:T(8,128)(2,1)S(1)}, u32[]{:S(2)}, u32[]{:S(2)}) collective-permute-start(bf16[2,64,2048]{2,1,0:T(8,128)(2,1)S(1)} %copy-done.21), channel_id=1, source_target_pairs={{80,0},{81,1},{82,2},{83,3},{84,4},{85,5},{86,6},{87,7},{88,8},{89... | collective-permute-start | bytes 1572872 | tf_op jit(solution)/shard_map/ppermute | solution.py:477
  228.3 7.9 %combine.2.refs_5_ = f32[512,2048]{1,0:T(8,128)} custom-call(bf16[512,1408]{1,0:T(8,128)(2,1)} %get-tuple-element.57.share_ref, bf16[2,64,2048]{2,1,0:T(8,128)(2,1)} %get-tuple-element.63.refs_0_, bf16[2,64,2048]{2,1,0:T(8,128)(2,1)} %collective-permute-done.18.refs_1_, bf16[2,64,2048]{2,1,0:T(8,128)(2,1)} %copy-done.25, bf16[2,64,2048]{2,1,0:T(8,128)(2,1)} %copy-done.27, ...), custom_call_target="tpu_custom_call" | custom-call | flops 5905580032 | bytes 8388608 | tf_op jit(solution)/shard_map/combine/pallas_call | solution.py:414
  236.2 18.8 %collective-permute-done.12.refs_3_ = bf16[2,64,2048]{2,1,0:T(8,128)(2,1)S(1)} collective-permute-done((bf16[2,64,2048]{2,1,0:T(8,128)(2,1)S(1)}, bf16[2,64,2048]{2,1,0:T(8,128)(2,1)S(1)}, u32[]{:S(2)}, u32[]{:S(2)}) %collective-permute-start.12) | collective-permute-done | bytes 524320 | tf_op jit(solution)/shard_map/ppermute | solution.py:477
  260.3 6.3 %combine.3 = bf16[512,2048]{1,0:T(8,128)(2,1)} custom-call(bf16[512,640]{1,0:T(8,128)(2,1)} %get-tuple-element.45.share_ref, bf16[2,64,2048]{2,1,0:T(8,128)(2,1)} %copy-done.32, bf16[2,64,2048]{2,1,0:T(8,128)(2,1)} %copy-done.26, bf16[2,64,2048]{2,1,0:T(8,128)(2,1)} %copy-done.29, bf16[2,64,2048]{2,1,0:T(8,128)(2,1)} %copy-done.30, ...), custom_call_target="tpu_custom_call" | custom-call | flops 2684354560 | bytes 8388608 | tf_op jit(solution)/shard_map/combine/pallas_call | solution.py:414
  266.6 147.1 %attend.2 = (f32[2048,128]{1,0:T(8,128)}, f32[2048,256]{1,0:T(8,128)}) custom-call(f32[1]{0:T(128)} %bitcast.safe_ref, bf16[2048,256]{1,0:T(8,128)(2,1)} %query.1.q_ref, bf16[8192,256]{1,0:T(8,128)(2,1)} %pad_maximum_fusion.kv_ref), custom_call_target="tpu_custom_call" | custom-call | flops 17179869184 | bytes 4194304 | tf_op jit(solution)/shard_map/attend/pallas_call | solution.py:194
  413.7 147.5 %attend.3 = bf16[128,1024]{1,0:T(8,128)(2,1)} custom-call(f32[1]{0:T(128)} %bitcast.safe_ref, bf16[2048,256]{1,0:T(8,128)(2,1)} %query.1.q_ref, bf16[8192,256]{1,0:T(8,128)(2,1)} %collective-permute-done.3.kv_ref, f32[2048,128]{1,0:T(8,128)} %get-tuple-element.41.refs_0_, f32[2048,256]{1,0:T(8,128)} %get-tuple-element.42.refs_1_), custom_call_target="tpu_custom_call" | custom-call | flops 17179869184 | bytes 4194304 | tf_op jit(solution)/shard_map/attend/pallas_call | solution.py:194
  (138 shorter events, 68.9 us)
Async XLA Ops:
  4.9 51.5 %all-to-all-start = ((bf16[16,128,256]{2,1,0:T(8,128)(2,1)}), bf16[16,128,256]{2,1,0:T(8,128)(2,1)S(1)}, u32[]{:S(2)}, u32[]{:S(2)}) async-start(bf16[16,128,256]{2,1,0:T(8,128)(2,1)} %keyval.1), calls=%async_computation | async-start | bytes 2097152 | tf_op jit(solution)/shard_map/all_to_all | solution.py:486
  32.6 23.8 %collective-permute-start.24 = (bf16[2,64,2048]{2,1,0:T(8,128)(2,1)}, bf16[2,64,2048]{2,1,0:T(8,128)(2,1)S(1)}, u32[]{:S(2)}, u32[]{:S(2)}) collective-permute-start(bf16[2,64,2048]{2,1,0:T(8,128)(2,1)} %get-tuple-element.70), channel_id=1, source_target_pairs={{0,40},{1,41},{2,42},{3,43},{4,44},{5,45},{6,46},{7,47},{8,48},{9,... | collective-permute-start | bytes 1572872 | tf_op jit(solution)/shard_map/ppermute | solution.py:477
  33.2 24.5 %collective-permute-start.25 = (bf16[2,64,2048]{2,1,0:T(8,128)(2,1)}, bf16[2,64,2048]{2,1,0:T(8,128)(2,1)}, u32[]{:S(2)}, u32[]{:S(2)}) collective-permute-start(bf16[2,64,2048]{2,1,0:T(8,128)(2,1)} %get-tuple-element.71), channel_id=1, source_target_pairs={{0,120},{1,121},{2,122},{3,123},{4,124},{5,125},{6,126},{7,127},{8... | collective-permute-start | bytes 1572872 | tf_op jit(solution)/shard_map/ppermute | solution.py:477
  37.9 29.5 %collective-permute-start.26 = (bf16[2,64,2048]{2,1,0:T(8,128)(2,1)}, bf16[2,64,2048]{2,1,0:T(8,128)(2,1)}, u32[]{:S(2)}, u32[]{:S(2)}) collective-permute-start(bf16[2,64,2048]{2,1,0:T(8,128)(2,1)} %get-tuple-element.72), channel_id=1, source_target_pairs={{0,56},{1,105},{2,58},{3,107},{4,60},{5,109},{6,62},{7,111},{8,32}... | collective-permute-start | bytes 1572872 | tf_op jit(solution)/shard_map/ppermute | solution.py:477
  41.4 26.5 %collective-permute-start.27 = (bf16[2,64,2048]{2,1,0:T(8,128)(2,1)}, bf16[2,64,2048]{2,1,0:T(8,128)(2,1)}, u32[]{:S(2)}, u32[]{:S(2)}) collective-permute-start(bf16[2,64,2048]{2,1,0:T(8,128)(2,1)} %get-tuple-element.73), channel_id=1, source_target_pairs={{0,104},{1,57},{2,106},{3,59},{4,108},{5,61},{6,110},{7,63},{8,112... | collective-permute-start | bytes 1572872 | tf_op jit(solution)/shard_map/ppermute | solution.py:477
  46.8 24.7 %collective-permute-start.14 = (bf16[2,64,2048]{2,1,0:T(8,128)(2,1)}, bf16[2,64,2048]{2,1,0:T(8,128)(2,1)S(1)}, u32[]{:S(2)}, u32[]{:S(2)}) collective-permute-start(bf16[2,64,2048]{2,1,0:T(8,128)(2,1)} %get-tuple-element.59), channel_id=1, source_target_pairs={{0,8},{1,33},{2,10},{3,35},{4,12},{5,37},{6,14},{7,39},{8,16},{9,4... | collective-permute-start | bytes 1572872 | tf_op jit(solution)/shard_map/ppermute | solution.py:477
  56.4 47.2 %collective-permute-start = (bf16[2048,256]{1,0:T(8,128)(2,1)S(1)}, bf16[2048,256]{1,0:T(8,128)(2,1)S(1)}, u32[]{:S(2)}, u32[]{:S(2)}) collective-permute-start(bf16[2048,256]{1,0:T(8,128)(2,1)S(1)} %bitcast.14), channel_id=1, source_target_pairs={{0,2},{1,3},{2,4},{3,5},{4,6},{5,7},{6,0},{7,1},{8,10},{9,11},{10,... | collective-permute-start | bytes 3145736 | tf_op jit(solution)/shard_map/ppermute | solution.py:491
  57.7 49.2 %collective-permute-start.1 = (bf16[2048,256]{1,0:T(8,128)(2,1)S(1)}, bf16[2048,256]{1,0:T(8,128)(2,1)S(1)}, u32[]{:S(2)}, u32[]{:S(2)}) collective-permute-start(bf16[2048,256]{1,0:T(8,128)(2,1)S(1)} %bitcast.15), channel_id=1, source_target_pairs={{0,4},{1,5},{2,6},{3,7},{4,0},{5,1},{6,2},{7,3},{8,12},{9,13},{10,... | collective-permute-start | bytes 3145736 | tf_op jit(solution)/shard_map/ppermute | solution.py:491
  67.4 41.8 %collective-permute-start.2 = (bf16[2048,256]{1,0:T(8,128)(2,1)S(1)}, bf16[2048,256]{1,0:T(8,128)(2,1)S(1)}, u32[]{:S(2)}, u32[]{:S(2)}) collective-permute-start(bf16[2048,256]{1,0:T(8,128)(2,1)S(1)} %bitcast.16), channel_id=1, source_target_pairs={{0,6},{1,7},{2,0},{3,1},{4,2},{5,3},{6,4},{7,5},{8,14},{9,15},{10,... | collective-permute-start | bytes 3145736 | tf_op jit(solution)/shard_map/ppermute | solution.py:491
  77.7 33.8 %collective-permute-start.17 = (bf16[2,64,2048]{2,1,0:T(8,128)(2,1)S(1)}, bf16[2,64,2048]{2,1,0:T(8,128)(2,1)S(1)}, u32[]{:S(2)}, u32[]{:S(2)}) collective-permute-start(bf16[2,64,2048]{2,1,0:T(8,128)(2,1)S(1)} %copy-done.15), channel_id=1, source_target_pairs={{0,96},{1,25},{2,98},{3,27},{4,100},{5,29},{6,102},{7,31},{8,104},... | collective-permute-start | bytes 1572872 | tf_op jit(solution)/shard_map/ppermute | solution.py:477
  82.1 39.4 %collective-permute-start.4 = (bf16[2,64,2048]{2,1,0:T(8,128)(2,1)}, bf16[2,64,2048]{2,1,0:T(8,128)(2,1)S(1)}, u32[]{:S(2)}, u32[]{:S(2)}) collective-permute-start(bf16[2,64,2048]{2,1,0:T(8,128)(2,1)} %get-tuple-element.47), channel_id=1, source_target_pairs={{0,80},{1,81},{2,82},{3,83},{4,84},{5,85},{6,86},{7,87},{8,88},{9,... | collective-permute-start | bytes 1572872 | tf_op jit(solution)/shard_map/ppermute | solution.py:477
  103.6 23.6 %collective-permute-start.5 = (bf16[2,64,2048]{2,1,0:T(8,128)(2,1)}, bf16[2,64,2048]{2,1,0:T(8,128)(2,1)S(1)}, u32[]{:S(2)}, u32[]{:S(2)}) collective-permute-start(bf16[2,64,2048]{2,1,0:T(8,128)(2,1)} %get-tuple-element.48), channel_id=1, source_target_pairs={{0,48},{1,73},{2,50},{3,75},{4,52},{5,77},{6,54},{7,79},{8,56},{9,... | collective-permute-start | bytes 1572872 | tf_op jit(solution)/shard_map/ppermute | solution.py:477
  106.9 41.6 %collective-permute-start.6 = (bf16[2,64,2048]{2,1,0:T(8,128)(2,1)}, bf16[2,64,2048]{2,1,0:T(8,128)(2,1)S(1)}, u32[]{:S(2)}, u32[]{:S(2)}) collective-permute-start(bf16[2,64,2048]{2,1,0:T(8,128)(2,1)} %get-tuple-element.49), channel_id=1, source_target_pairs={{0,112},{1,89},{2,114},{3,91},{4,116},{5,93},{6,118},{7,95},{8,120... | collective-permute-start | bytes 1572872 | tf_op jit(solution)/shard_map/ppermute | solution.py:477
  109.3 50.5 %collective-permute-start.7 = (bf16[2,64,2048]{2,1,0:T(8,128)(2,1)}, bf16[2,64,2048]{2,1,0:T(8,128)(2,1)S(1)}, u32[]{:S(2)}, u32[]{:S(2)}) collective-permute-start(bf16[2,64,2048]{2,1,0:T(8,128)(2,1)} %get-tuple-element.50), channel_id=1, source_target_pairs={{0,72},{1,49},{2,74},{3,51},{4,76},{5,53},{6,78},{7,55},{8,80},{9,... | collective-permute-start | bytes 1572872 | tf_op jit(solution)/shard_map/ppermute | solution.py:477
  111.5 302.2 %collective-permute-start.3 = (bf16[8192,256]{1,0:T(8,128)(2,1)}, bf16[8192,256]{1,0:T(8,128)(2,1)}, u32[]{:S(2)}, u32[]{:S(2)}) collective-permute-start(bf16[8192,256]{1,0:T(8,128)(2,1)} %pad_maximum_fusion.kv_ref), channel_id=1, source_target_pairs={{0,1},{1,0},{2,3},{3,2},{4,5},{5,4},{6,7},{7,6},{8,9},{9,8},{10,11... | collective-permute-start | bytes 12582920 | tf_op jit(solution)/shard_map/ppermute | solution.py:493
  121.5 47.2 %collective-permute-start.8 = (bf16[2,64,2048]{2,1,0:T(8,128)(2,1)S(1)}, bf16[2,64,2048]{2,1,0:T(8,128)(2,1)S(1)}, u32[]{:S(2)}, u32[]{:S(2)}) collective-permute-start(bf16[2,64,2048]{2,1,0:T(8,128)(2,1)S(1)} %copy-done.12), channel_id=1, source_target_pairs={{0,88},{1,113},{2,90},{3,115},{4,92},{5,117},{6,94},{7,119},{8,64}... | collective-permute-start | bytes 1572872 | tf_op jit(solution)/shard_map/ppermute | solution.py:477
  127.2 44.3 %collective-permute-start.28 = (bf16[2,64,2048]{2,1,0:T(8,128)(2,1)}, bf16[2,64,2048]{2,1,0:T(8,128)(2,1)S(1)}, u32[]{:S(2)}, u32[]{:S(2)}) collective-permute-start(bf16[2,64,2048]{2,1,0:T(8,128)(2,1)} %get-tuple-element.74), channel_id=1, source_target_pairs={{16,0},{65,1},{18,2},{67,3},{20,4},{69,5},{22,6},{71,7},{24,8},{73... | collective-permute-start | bytes 1572872 | tf_op jit(solution)/shard_map/ppermute | solution.py:477
  148.5 23.0 %collective-permute-start.29 = (bf16[2,64,2048]{2,1,0:T(8,128)(2,1)}, bf16[2,64,2048]{2,1,0:T(8,128)(2,1)S(1)}, u32[]{:S(2)}, u32[]{:S(2)}) collective-permute-start(bf16[2,64,2048]{2,1,0:T(8,128)(2,1)} %get-tuple-element.75), channel_id=1, source_target_pairs={{64,0},{17,1},{66,2},{19,3},{68,4},{21,5},{70,6},{23,7},{72,8},{25... | collective-permute-start | bytes 1572872 | tf_op jit(solution)/shard_map/ppermute | solution.py:477
  192.4 26.6 %collective-permute-start.21 = (bf16[2,64,2048]{2,1,0:T(8,128)(2,1)}, bf16[2,64,2048]{2,1,0:T(8,128)(2,1)S(1)}, u32[]{:S(2)}, u32[]{:S(2)}) collective-permute-start(bf16[2,64,2048]{2,1,0:T(8,128)(2,1)} %get-tuple-element.67), channel_id=1, source_target_pairs={{96,0},{25,1},{98,2},{27,3},{100,4},{29,5},{102,6},{31,7},{104,8},... | collective-permute-start | bytes 1572872 | tf_op jit(solution)/shard_map/ppermute | solution.py:477
  193.7 25.3 %collective-permute-start.10 = (bf16[2,64,2048]{2,1,0:T(8,128)(2,1)}, bf16[2,64,2048]{2,1,0:T(8,128)(2,1)S(1)}, u32[]{:S(2)}, u32[]{:S(2)}) collective-permute-start(bf16[2,64,2048]{2,1,0:T(8,128)(2,1)} %get-tuple-element.53), channel_id=1, source_target_pairs={{48,0},{73,1},{50,2},{75,3},{52,4},{77,5},{54,6},{79,7},{56,8},{81... | collective-permute-start | bytes 1572872 | tf_op jit(solution)/shard_map/ppermute | solution.py:477
  209.7 26.5 %collective-permute-start.11 = (bf16[2,64,2048]{2,1,0:T(8,128)(2,1)S(1)}, bf16[2,64,2048]{2,1,0:T(8,128)(2,1)S(1)}, u32[]{:S(2)}, u32[]{:S(2)}) collective-permute-start(bf16[2,64,2048]{2,1,0:T(8,128)(2,1)S(1)} %copy-done.24), channel_id=1, source_target_pairs={{112,0},{89,1},{114,2},{91,3},{116,4},{93,5},{118,6},{95,7},{120,8... | collective-permute-start | bytes 1572872 | tf_op jit(solution)/shard_map/ppermute | solution.py:477
  210.1 45.0 %collective-permute-start.12 = (bf16[2,64,2048]{2,1,0:T(8,128)(2,1)S(1)}, bf16[2,64,2048]{2,1,0:T(8,128)(2,1)S(1)}, u32[]{:S(2)}, u32[]{:S(2)}) collective-permute-start(bf16[2,64,2048]{2,1,0:T(8,128)(2,1)S(1)} %copy-done.23), channel_id=1, source_target_pairs={{72,0},{49,1},{74,2},{51,3},{76,4},{53,5},{78,6},{55,7},{80,8},{57... | collective-permute-start | bytes 1572872 | tf_op jit(solution)/shard_map/ppermute | solution.py:477
  219.0 40.3 %collective-permute-start.13 = (bf16[2,64,2048]{2,1,0:T(8,128)(2,1)S(1)}, bf16[2,64,2048]{2,1,0:T(8,128)(2,1)S(1)}, u32[]{:S(2)}, u32[]{:S(2)}) collective-permute-start(bf16[2,64,2048]{2,1,0:T(8,128)(2,1)S(1)} %copy-done.22), channel_id=1, source_target_pairs={{88,0},{113,1},{90,2},{115,3},{92,4},{117,5},{94,6},{119,7},{64,8}... | collective-permute-start | bytes 1572872 | tf_op jit(solution)/shard_map/ppermute | solution.py:477
  219.1 40.2 %collective-permute-start.9 = (bf16[2,64,2048]{2,1,0:T(8,128)(2,1)S(1)}, bf16[2,64,2048]{2,1,0:T(8,128)(2,1)S(1)}, u32[]{:S(2)}, u32[]{:S(2)}) collective-permute-start(bf16[2,64,2048]{2,1,0:T(8,128)(2,1)S(1)} %copy-done.21), channel_id=1, source_target_pairs={{80,0},{81,1},{82,2},{83,3},{84,4},{85,5},{86,6},{87,7},{88,8},{89... | collective-permute-start | bytes 1572872 | tf_op jit(solution)/shard_map/ppermute | solution.py:477
  (44 other events, 959.3 us)
